TPU v7x, 256 devices: a 4x2x16 block of a 4x16x16 slice. The times are simulated.
256 devices in a mesh: grp: 2 (over y), fs: 16 (over z), tp: 8 (over x, core).
Axes of the slice: x: 4, y: 2, z: 16, core: 2. Of those that a mesh axis runs over, the one named last changes fastest.
The devices are a block of a 4x16x16 slice.
Arguments:
- tokens: bfloat16 [32768, 2048], P(('grp', 'fs'), 'tp'), parts along dimension 0, may hold values from -6 to 6
- norm1_gain: float32 [2048], replicated, may hold values from 0.1 to 1.9
- weight_u: float32 [2048, 1024], P('fs', 'tp'), may hold values from -0.125 to 0.125
- weight_v: float32 [2048, 1024], P('fs', 'tp'), may hold values from -0.125 to 0.125
- scale_u: float32 [1024], P('tp'), may hold values from 0.5 to 2
- scale_v: float32 [1024], P('tp'), may hold values from 0.05 to 4.5
- mix_gain: float32 [1024], P('tp'), may hold values from 0.1 to 1.9
- spatial_weight: float32 [4, 128, 128], replicated, may hold values from -0.5 to 0.5
- spatial_bias: float32 [4, 128], replicated, may hold values from 0.5 to 1.5
- weight_out: float32 [1024, 2048], P('tp', 'fs'), may hold values from -0.1875 to 0.1875
- scale_out: float32 [2048], P('fs'), may hold values from 0.5 to 2
- norm2_gain: float32 [2048], replicated, may hold values from 0.1 to 1.9
- weight_up: float32 [2048, 8192], P('fs', 'tp'), may hold values from -0.125 to 0.125
- scale_up: float32 [8192], P('tp'), may hold values from 0.5 to 2
- weight_down: float32 [8192, 2048], P('tp', 'fs'), may hold values from -0.0625 to 0.0625
- scale_down: float32 [2048], P('fs'), may hold values from 0.5 to 2
Outputs:
- result: bfloat16 [32768, 2048], P(('grp', 'fs'), 'tp'), parts along dimension 0
There are 2 independent parts, one for each index of `grp`. A program takes and returns all parts, laid end to end along the dimension named above; an argument that names none is the same for every part. Nothing has to cross between parts.
All inputs are finite; a program needn't handle non-finite values.
Results may differ from a plain program's by a relative error of at most 0.023.
Values may be sent and summed in bfloat16 or wider, within the bound.
A program may use at most 128 MiB of HBM per device.

v0:
```python
import jax
import jax.numpy as jnp
from jax import lax
from jax.sharding import PartitionSpec as P

GM_W = 1024
GROUPS = 4
BLOCK = 128


def rows_first(arrays, axis, dims):
    turned = [jnp.moveaxis(a, dim, 0) for a, dim in zip(arrays, dims)]
    both = jnp.concatenate([t.reshape(len(t), -1) for t in turned], axis=1)
    whole, at, finished = (lax.all_gather(both, axis, axis=0, tiled=True), 0, [])
    for t, dim in zip(turned, dims):
        share = whole[:, at : at + t[0].size].reshape(-1, *t.shape[1:])
        finished.append(jnp.moveaxis(share, 0, dim))
        at += t[0].size
    return tuple(finished)


def in_one_piece(arrays, axis, dim, along):
    widths = [a.shape[along] for a in arrays]
    both = jnp.concatenate(arrays, axis=along)
    whole = lax.all_gather(both, axis, axis=dim, tiled=True)
    return tuple(jnp.split(whole, [sum(widths[:k]) for k in range(1, len(widths))], axis=along))


def from_everyone(shard, axis):
    peers = lax.axis_size(axis)
    return lax.all_to_all(
        jnp.broadcast_to(shard[None], (peers, *shard.shape)), axis, 0, 0, tiled=True
    )


def taken_together(shard, axis):
    return from_everyone(shard, axis).sum(axis=0)


def packed_total(arrays, axis):
    ends = [0]
    for a in arrays:
        ends.append(ends[-1] + a.size)
    total = taken_together(jnp.concatenate([a.ravel() for a in arrays]), axis)
    return tuple((total[b:e].reshape(a.shape) for a, b, e in zip(arrays, ends, ends[1:])))


def laid_out(parts, dim):
    dims = list(parts.shape[1:])
    dims[dim] *= parts.shape[0]
    return jnp.moveaxis(parts, 0, dim).reshape(dims)


def gather_directly(shard, axis, dim):
    parts = from_everyone(shard, axis)
    return laid_out(parts, dim)


def split_up(shard, dim, peers):
    dims = shard.shape
    parts = shard.reshape(*dims[:dim], peers, dims[dim] // peers, *dims[dim + 1 :])
    return jnp.moveaxis(parts, dim, 0)


def sent_and_summed(shard, axis, dim):
    parts = split_up(shard, dim, lax.axis_size(axis))
    arrived = lax.all_to_all(parts, axis, split_axis=0, concat_axis=0, tiled=True)
    return arrived.astype(jnp.float32).sum(axis=0)


def per_device(
    tokens,
    norm1_gain,
    weight_u,
    weight_v,
    scale_u,
    scale_v,
    mix_gain,
    spatial_weight,
    spatial_bias,
    weight_out,
    scale_out,
    norm2_gain,
    weight_up,
    scale_up,
    weight_down,
    scale_down,
):
    feature_count = norm1_gain.shape[0]
    out_scales, down_scales = rows_first((scale_out, scale_down), "fs", (0, 0))
    full_u, full_v = in_one_piece(
        (weight_u.astype(jnp.bfloat16), weight_v.astype(jnp.bfloat16)), "fs", 0, 1
    )
    widened_in = tokens.astype(jnp.float32)
    squares_in = taken_together(jnp.sum(widened_in * widened_in, axis=1), "tp")
    inverse_in = lax.rsqrt(squares_in / feature_count + 1e-06)[:, None]
    gain_piece = norm1_gain
    normed_piece = (
        lax.all_gather(tokens, "tp", axis=1, tiled=True).astype(jnp.float32)
        * inverse_in
        * gain_piece
    ).astype(jnp.bfloat16)
    pre_u = jnp.dot(normed_piece, full_u, preferred_element_type=jnp.float32)
    pre_v = jnp.dot(normed_piece, full_v, preferred_element_type=jnp.float32)
    gate_u = jax.nn.gelu(pre_u * scale_u)
    act_v = jax.nn.gelu(pre_v * scale_v)
    local_width = act_v.shape[1]
    row_sums, row_squares = packed_total(
        (jnp.sum(act_v, axis=1), jnp.sum(act_v * act_v, axis=1)), "tp"
    )
    row_mean = (row_sums / GM_W)[:, None]
    square = (row_squares / GM_W)[:, None]
    v_norm = (
        (act_v - row_mean) * lax.rsqrt(square - row_mean * row_mean + 1e-06) * mix_gain
    ).astype(jnp.bfloat16)
    group_index = lax.axis_index("tp") * local_width // (GM_W // GROUPS)
    lower_mask = jnp.tril(jnp.ones((BLOCK, BLOCK), jnp.float32))
    spatial_mask = (
        lax.dynamic_index_in_dim(spatial_weight, group_index, 0, keepdims=False) * lower_mask
    ).astype(jnp.bfloat16)
    block_bias = lax.dynamic_index_in_dim(spatial_bias, group_index, 0, keepdims=False)
    blocks = v_norm.reshape(-1, BLOCK, local_width)
    mixed_cols = jnp.einsum("ts,nsc->ntc", spatial_mask, blocks, preferred_element_type=jnp.float32)
    mixed_cols = mixed_cols + block_bias[None, :, None]
    gated = (gate_u * mixed_cols.reshape(-1, local_width)).astype(jnp.bfloat16)
    out_rounded = weight_out.astype(jnp.bfloat16)
    full_out = gather_directly(out_rounded, "fs", 1)
    columns = full_out
    piece_scale = out_scales
    product = lax.dot_general(
        columns, gated, (((0,), (1,)), ((), ())), preferred_element_type=jnp.float32
    )
    mixer_sum = sent_and_summed((product * piece_scale[:, None]).astype(jnp.bfloat16), "tp", 0).T
    residual = (tokens.astype(jnp.float32) + mixer_sum).astype(jnp.bfloat16)
    full_up = lax.all_gather(weight_up.astype(jnp.bfloat16), "fs", axis=0, tiled=True)
    widened_mid = residual.astype(jnp.float32)
    squares_mid = taken_together(jnp.sum(widened_mid * widened_mid, axis=1), "tp")
    inverse_mid = lax.rsqrt(squares_mid / feature_count + 1e-06)[:, None]
    gain_piece = norm2_gain
    normed_piece = (
        lax.all_gather(residual, "tp", axis=1, tiled=True).astype(jnp.float32)
        * inverse_mid
        * gain_piece
    ).astype(jnp.bfloat16)
    pre_up = jnp.dot(normed_piece, full_up, preferred_element_type=jnp.float32)
    hidden = jnp.square(jax.nn.relu(pre_up * scale_up)).astype(jnp.bfloat16)
    down_rounded = weight_down.astype(jnp.bfloat16)
    full_down = lax.all_gather(down_rounded, "fs", axis=1, tiled=True)
    columns = full_down
    piece_scale = down_scales
    product = lax.dot_general(
        columns, hidden, (((0,), (1,)), ((), ())), preferred_element_type=jnp.float32
    )
    channel_sum = sent_and_summed((product * piece_scale[:, None]).astype(jnp.bfloat16), "tp", 0).T
    return (residual.astype(jnp.float32) + channel_sum).astype(jnp.bfloat16)


def solution(mesh):
    placed = (
        P(("grp", "fs"), "tp"),
        P(),
        P("fs", "tp"),
        P("fs", "tp"),
        P("tp"),
        P("tp"),
        P("tp"),
        P(),
        P(),
        P("tp", "fs"),
        P("fs"),
        P(),
        P("fs", "tp"),
        P("tp"),
        P("tp", "fs"),
        P("fs"),
    )
    return jax.shard_map(
        per_device, mesh=mesh, in_specs=placed, out_specs=P(("grp", "fs"), "tp"), check_vma=False
    )
```

profile of v0, /device:TPU:33, one launch (start us, length us, event | category | flops | bytes accessed | tf_op | source)
XLA Modules:
  0.0 441.5 jit_solution(2833319053719733475)
XLA Ops:
  9.8 1.8 convert_element_type.91
  11.7 1.8 convert_element_type.93
  13.6 1.3 fusion.5
  14.9 27.6 %all_to_all.33 = f32[8,1,1024]{2,1,0:T(1,128)S(1)} all-to-all(f32[8,1,1024]{2,1,0:T(1,128)S(1)} %broadcast_in_dim.13), channel_id=1, replica_groups=mesh['grp'=2,'fs'=16,'tp'=8] {'tp'}, dimensions={0} | all-to-all | bytes 65536 | tf_op jit(solution)/shard_map/all_to_all | solution.py:31
  42.6 39.5 %all-gather.8.cloned.1.call-done = bf16[2048,256]{1,0:T(8,128)(2,1)} async-done(((bf16[128,256]{1,0:T(8,128)(2,1)}), bf16[2048,256]{1,0:T(8,128)(2,1)}) %all-gather.8.cloned.1.call-update) | async-done | bytes 1048592 | tf_op jit(solution)/shard_map/all_gather | solution.py:25
  82.0 51.7 %all-gather.6.cloned.1.call-done = bf16[1024,2048]{1,0:T(8,128)(2,1)} async-done(((bf16[1024,256]{1,0:T(8,128)(2,1)}), bf16[1024,2048]{1,0:T(8,128)(2,1)}) %all-gather.6.cloned.1.call-update) | async-done | bytes 4194320 | tf_op jit(solution)/shard_map/all_gather | solution.py:99
  133.8 3.8 fusion.48
  138.2 4.2 all-to-all-start.1
  142.6 4.7 %all-to-all-done.1 = f32[8,1,2048]{2,1,0:T(1,128)S(1)} async-done(((f32[8,1,2048]{2,1,0:T(1,128)}), f32[8,1,2048]{2,1,0:T(1,128)S(1)}, u32[]{:S(2)}, u32[]{:S(2)}) %all-to-all-start.1) | async-done | bytes 65568 | tf_op jit(solution)/shard_map/all_to_all | solution.py:31
  147.3 0.9 broadcast_in_dim.18
  148.2 12.1 %all-to-all-start.2 = ((bf16[16,128,128]{1,2,0:T(8,128)(2,1)}), bf16[16,128,128]{1,2,0:T(8,128)(2,1)S(1)}, u32[]{:S(2)}, u32[]{:S(2)}) async-start(bf16[16,128,128]{1,2,0:T(8,128)(2,1)} %broadcast_in_dim.18), calls=%async_computation.2 | async-start | bytes 1048576 | tf_op jit(solution)/shard_map/all_to_all | solution.py:31
  160.4 50.6 %all_gather.20 = f32[2048,2]{0,1:T(2,128)S(1)} all-gather(f32[128,2]{0,1:T(2,128)S(1)} %pad_maximum_fusion.2), channel_id=1, replica_groups=mesh['grp'=2,'fs'=16,'tp'=8] {'fs'}, dimensions={0}, use_global_device_ids=true | all-gather | bytes 17408 | tf_op jit(solution)/shard_map/all_gather | solution.py:14
  211.5 1.1 convolution_add_fusion
  212.6 8.6 %multiply_convert_fusion.2 = bf16[1024,2048]{1,0:T(8,128)(2,1)} fusion(bf16[128,2048]{0,1:T(8,128)(2,1)S(1)} %bitcast.41, f32[2048]{0:T(1024)S(1)} %bitcast.44, f32[1024,128]{1,0:T(8,128)S(1)} %bitcast.42, bf16[1024,2048]{1,0:T(8,128)(2,1)} %all-gather.6.cloned.1.call-done, f32[2048]{0:T(1024)S(1)} %copy-done.8, f32[1024]{0:T(1024)S(1)} %add_rsqrt_fusion.1, ...), kind=kOutput, calls=%fused_computation.4 | convolution fusion | flops 1087766528 | bytes 9982464 | tf_op jit(solution)/shard_map/dot_general | solution.py:130
  221.2 2.5 copy.40
  223.6 56.0 %all_to_all.34 = bf16[8,256,1024]{1,2,0:T(8,128)(2,1)S(1)} all-to-all(bf16[8,256,1024]{1,2,0:T(8,128)(2,1)S(1)} %bitcast.36), channel_id=1, replica_groups=mesh['grp'=2,'fs'=16,'tp'=8] {'tp'}, dimensions={0} | all-to-all | bytes 8388608 | tf_op jit(solution)/shard_map/all_to_all | solution.py:67
  280.7 1.0 fusion.7
  281.7 8.2 %all_to_all.35 = f32[8,1,1024]{2,1,0:T(1,128)S(1)} all-to-all(f32[8,1,1024]{2,1,0:T(1,128)S(1)} %broadcast_in_dim.19), channel_id=1, replica_groups=mesh['grp'=2,'fs'=16,'tp'=8] {'tp'}, dimensions={0} | all-to-all | bytes 65536 | tf_op jit(solution)/shard_map/all_to_all | solution.py:31
  290.1 24.2 %all-gather.14.cloned.1.call-done = bf16[1024,2048]{1,0:T(8,128)(2,1)} async-done(((bf16[1024,128]{1,0:T(8,128)(2,1)}), bf16[1024,2048]{1,0:T(8,128)(2,1)}) %all-gather.14.cloned.1.call-update) | async-done | bytes 4194320 | tf_op jit(solution)/shard_map/all_gather | solution.py:148
  314.3 48.9 %all-gather.10.cloned.1.call-done = bf16[1024,2048]{1,0:T(8,128)(2,1)} async-done(((bf16[1024,256]{1,0:T(8,128)(2,1)}), bf16[1024,2048]{1,0:T(8,128)(2,1)}) %all-gather.10.cloned.1.call-update) | async-done | bytes 4194320 | tf_op jit(solution)/shard_map/all_gather | solution.py:141
  363.2 14.7 %multiply_convert_fusion = bf16[1024,2048]{1,0:T(8,128)(2,1)} fusion(bf16[1024,2048]{1,0:T(8,128)(2,1)} %all-gather.14.cloned.1.call-done, f32[2048]{0:T(1024)S(1)} %bitcast.43, f32[1024]{0:T(1024)S(1)} %copy-done.10, bf16[2048,1024]{1,0:T(8,128)(2,1)} %all-gather.12.cloned.1.call-done, bf16[1024,2048]{1,0:T(8,128)(2,1)} %all-gather.10.cloned.1.call-done, ...), kind=kOutput, calls=%fused_computation.1 | convolution fusion | flops 8606711808 | bytes 16801792 | tf_op jit(solution)/shard_map/dot_general | solution.py:151
  377.8 2.5 copy.39
  380.3 52.7 %all_to_all.36 = bf16[8,256,1024]{1,2,0:T(8,128)(2,1)S(1)} all-to-all(bf16[8,256,1024]{1,2,0:T(8,128)(2,1)S(1)} %bitcast.37), channel_id=1, replica_groups=mesh['grp'=2,'fs'=16,'tp'=8] {'tp'}, dimensions={0} | all-to-all | bytes 8388608 | tf_op jit(solution)/shard_map/all_to_all | solution.py:67
  434.0 0.9 fusion.8
  (57 shorter events, 7.0 us)
Async XLA Ops:
  6.5 204.5 %copy-start = (f32[4,128]{1,0:T(4,128)S(1)}, f32[4,128]{1,0:T(4,128)}, u32[]{:S(2)}) copy-start(f32[4,128]{1,0:T(4,128)} %param.24) | copy-start | bytes 6148
  6.6 75.5 %all-gather.8.cloned.1.call-start = ((), (), s32[]{:S(2)}) async-start(), calls=%async_computation.7 | async-start | bytes 1114112 | tf_op jit(solution)/shard_map/all_gather | solution.py:25
  9.0 124.8 %all-gather.6.cloned.1.call-start = ((), (), s32[]{:S(2)}) async-start(), calls=%async_computation.6 | async-start | bytes 4718592 | tf_op jit(solution)/shard_map/all_gather | solution.py:99
  9.8 280.3 %all-gather.12.cloned.1.call-start = ((), (), s32[]{:S(2)}) async-start(), calls=%async_computation.9 | async-start | bytes 4456448 | tf_op jit(solution)/shard_map/all_gather | solution.py:135
  11.7 302.6 %all-gather.14.cloned.1.call-start = ((), (), s32[]{:S(2)}) async-start(), calls=%async_computation.10 | async-start | bytes 4456448 | tf_op jit(solution)/shard_map/all_gather | solution.py:148
  42.5 100.0 %copy-start.3 = (f32[128,128]{1,0:T(8,128)S(1)}, f32[128,128]{1,0:T(8,128)}, u32[]{:S(2)}) copy-start(f32[128,128]{1,0:T(8,128)} %param.25) | copy-start | bytes 196612
  42.5 117.9 %copy-start.4 = (f32[128]{0:T(128)S(1)}, f32[128]{0:T(128)}, u32[]{:S(2)}) copy-start(f32[128]{0:T(128)} %param.31) | copy-start | bytes 1540
  42.5 117.9 %copy-start.5 = (f32[128]{0:T(128)S(1)}, f32[128]{0:T(128)}, u32[]{:S(2)}) copy-start(f32[128]{0:T(128)} %param.26) | copy-start | bytes 1540
  42.5 168.6 %copy-start.6 = (f32[128]{0:T(128)S(1)}, f32[128]{0:T(128)}, u32[]{:S(2)}) copy-start(f32[128]{0:T(128)} %param.22) | copy-start | bytes 1540
  42.5 170.0 %copy-start.8 = (f32[2048]{0:T(1024)S(1)}, f32[2048]{0:T(1024)}, u32[]{:S(2)}) copy-start(f32[2048]{0:T(1024)} %param.17) | copy-start | bytes 24580
  42.5 170.0 %copy-start.11 = (f32[128]{0:T(128)S(1)}, f32[128]{0:T(128)}, u32[]{:S(2)}) copy-start(f32[128]{0:T(128)} %param.20) | copy-start | bytes 1540
  82.0 130.6 %copy-start.7 = (bf16[2048,256]{1,0:T(8,128)(2,1)S(1)}, bf16[2048,256]{1,0:T(8,128)(2,1)}, u32[]{:S(2)}) copy-start(bf16[2048,256]{1,0:T(8,128)(2,1)} %all-gather.8.cloned.1.call-done) | copy-start | bytes 3145732
  138.2 9.1 %all-to-all-start.1 = ((f32[8,1,2048]{2,1,0:T(1,128)}), f32[8,1,2048]{2,1,0:T(1,128)S(1)}, u32[]{:S(2)}, u32[]{:S(2)}) async-start(f32[8,1,2048]{2,1,0:T(1,128)} %broadcast_in_dim.14), calls=%async_computation.1 | async-start | bytes 131072 | tf_op jit(solution)/shard_map/all_to_all | solution.py:31
  148.2 64.3 %all-to-all-start.2 = ((bf16[16,128,128]{1,2,0:T(8,128)(2,1)}), bf16[16,128,128]{1,2,0:T(8,128)(2,1)S(1)}, u32[]{:S(2)}, u32[]{:S(2)}) async-start(bf16[16,128,128]{1,2,0:T(8,128)(2,1)} %broadcast_in_dim.18), calls=%async_computation.2 | async-start | bytes 1048576 | tf_op jit(solution)/shard_map/all_to_all | solution.py:31
  160.3 202.9 %all-gather.10.cloned.1.call-start = ((), (), s32[]{:S(2)}) async-start(), calls=%async_computation.8 | async-start | bytes 4718592 | tf_op jit(solution)/shard_map/all_gather | solution.py:141
  279.6 1.1 copy-start.1
  279.6 83.6 %copy-start.9 = (f32[2048]{0:T(1024)S(1)}, f32[2048]{0:T(1024)}, u32[]{:S(2)}) copy-start(f32[2048]{0:T(1024)} %param.27) | copy-start | bytes 24580
  279.6 83.6 %copy-start.10 = (f32[1024]{0:T(1024)S(1)}, f32[1024]{0:T(1024)}, u32[]{:S(2)}) copy-start(f32[1024]{0:T(1024)} %param.29) | copy-start | bytes 12292
  433.0 1.0 copy-start.2
Sparse Core Ops, SparseCore 0:
  9.1 72.8 all-gather.7
  83.9 49.8 all-gather.5
  135.6 89.9 all-gather.11
  227.2 87.0 all-gather.13
  316.0 47.1 all-gather.9
where the time goes:
time: 442 us; the launch traced here: 441 us
  blocking collectives  195 us (44%)
  waiting for transfers between devices  170 us (38%)
  matrix products  28.1 us (6%)
  starting transfers between devices  16.6 us (4%)
  between operations  13.4 us (3%)
  other arithmetic  10.7 us (2%)
  local copies, waits for them, and re-layouts  7.6 us (2%)
    all_to_all x2, blocking collectives, sent_and_summed(): lax.all_to_all(parts, axis, split_axis=0, concat_axis=0, tiled=True)  109 us
    all_gather x1, waiting for transfers between devices, per_device(): lax.all_gather(tokens, 'tp', axis=1, tiled=True).astype(jnp.float32)  51.7 us
    all_gather x1, blocking collectives, rows_first(): lax.all_gather(both, axis, axis=0, tiled=True)  50.6 us
    all_gather x1, waiting for transfers between devices, per_device(): lax.all_gather(residual, 'tp', axis=1, tiled=True).astype(jnp.float32)  48.9 us
    all_gather x1, waiting for transfers between devices, in_one_piece(): whole = lax.all_gather(both, axis, axis=dim, tiled=True)  39.5 us
    all_to_all x2, blocking collectives, from_everyone(): lax.all_to_all(jnp.broadcast_to(shard[None], (peers, *shard.shape)), axis...  35.8 us
    all_gather x1, waiting for transfers between devices, per_device(): full_down = lax.all_gather(down_rounded, 'fs', axis=1, tiled=True)  24.2 us
    all_to_all x2, starting transfers between devices, from_everyone(): lax.all_to_all(jnp.broadcast_to(shard[None], (peers, *shard.shape)), axis...  16.3 us
  transfers between devices with their start and end apart: 7, of which 5 were waited for; matrix products, arithmetic and copies ran while one was open for 6% of the time, Pallas kernels for 0%

commit v1 on v0

v1 whole, which is shorter than its diff:
```python
import functools

import jax
import jax.numpy as jnp
from jax import lax
from jax.experimental import pallas as pl
from jax.experimental.pallas import tpu as pltpu
from jax.sharding import PartitionSpec as P

BF = jnp.bfloat16
F32 = jnp.float32
MESH = pl.DeviceIdType.MESH
EPS = 1e-06
CORES = 2
CHUNKS = 2
ROWS = 256


class Stream:
    def __init__(self, name, ref, rows, whole, paired):
        self.name, self.ref, self.rows, self.whole, self.paired = name, ref, rows, whole, paired


def kernel(
    dims,
    x_ref, g1_ref, wu_ref, wv_ref, suv_ref, mg_ref, sw_ref, sb_ref, wo_ref, so_ref,
    g2_ref, wup_ref, sup_ref, wdn_ref, sdn_ref,
    out_ref,
    wuv, wout, wup, wdn, xg, rg, ub, vt, st_own, st_p, st_c, st_x, gated, hid,
    ps1, pr1, qs1, op1, fi1, ps2, pr2, qs2, op2, fi2, mask, bias,
    z_recv, z_send, y_recv, y_send, ag_recv, ag_send, agp_recv, agp_send,
    rp_recv, rp_send, rr_recv, rr_send, st_recv, st_send,
):
    n_fs, n_tp = dims["fs"], dims["tp"]
    n_x = n_tp // CORES
    half_ring = n_fs // 2
    total_rows, width = x_ref.shape
    feats = width * n_tp
    u_w = wu_ref.shape[1]
    k_fs = wu_ref.shape[0]
    h_w = wup_ref.shape[1]
    gm_w = u_w * n_tp
    chunk = total_rows // CHUNKS
    half = chunk // 2
    block = sw_ref.shape[1]
    pair = dims["grp"] % 2 == 0

    g = lax.axis_index("grp")
    f = lax.axis_index("fs")
    t = lax.axis_index("tp")
    cx = t // CORES
    core = t % CORES
    par = g % 2

    def chip(d):
        return (cx + d) % n_x

    def tp_of(d):
        return chip(d) * CORES + core

    to_right, to_left, to_opp = {"tp": tp_of(1)}, {"tp": tp_of(n_x - 1)}, {"tp": tp_of(2)}
    to_mate = {"tp": cx * CORES + 1 - core}
    to_up, to_down = {"fs": (f + 1) % n_fs}, {"fs": (f + n_fs - 1) % n_fs}
    to_pair = {"grp": g + 1 - 2 * par}

    neighbours = [to_right, to_left, to_opp, to_mate, to_up, to_down]
    if pair:
        neighbours.append(to_pair)
    barrier = pltpu.get_barrier_semaphore()
    for n in neighbours:
        pl.semaphore_signal(barrier, inc=1, device_id=n, device_id_type=MESH)
    pl.semaphore_wait(barrier, len(neighbours))

    def rcopy(src, dst, ss, rs, dev):
        return pltpu.make_async_remote_copy(
            src_ref=src, dst_ref=dst, send_sem=ss, recv_sem=rs, device_id=dev, device_id_type=MESH)

    def got(ref, sem, spare, dev):
        rcopy(ref, ref, spare, sem, dev).wait_recv()

    def sent(ref, sem, spare, dev):
        rcopy(ref, ref, sem, spare, dev).wait_send()

    def rows_2d(ref, start):
        def at(slot, rows):
            return ref.at[pl.ds(pl.multiple_of(slot * k_fs + start, 16), rows), :]
        return at

    def rows_3d(ref, start):
        def at(slot, rows):
            return ref.at[slot, pl.ds(pl.multiple_of(start, 16), rows), :]
        return at

    def whole_2d(ref, rows):
        return ref.at[pl.ds(0, (n_fs - 1) * rows), :]

    def whole_3d(ref, rows):
        return ref.at[pl.ds(0, n_fs - 1), pl.ds(0, rows), :]

    def make(name, ref, three, own_rows, swap):
        at, whole = (rows_3d, whole_3d) if three else (rows_2d, whole_2d)
        result = []
        if pair and swap:
            shared = own_rows - 2 * swap
            result.append(Stream(name + "y", at(ref, par * (own_rows - swap)), swap, whole(ref, swap), True))
            result.append(Stream(name + "b", at(ref, swap), shared, whole(ref, shared), False))
        else:
            result.append(Stream(name, at(ref, 0), own_rows, whole(ref, own_rows), False))
        return result

    streams = {}
    for s in (make("uv", wuv, False, k_fs, 0) + make("out", wout, True, wo_ref.shape[0], 0)
              + make("up", wup, False, k_fs, 48) + make("dn", wdn, True, h_w, 416)):
        s.index = len(streams)
        streams[s.name] = s

    def z_dirs(s, hop):
        return (0, 1) if hop < half_ring else (s.index % 2,)

    def z_hop(name, hop):
        s = streams[name]
        for d in (0, 1):
            to = to_up if d == 0 else to_down
            if hop > 1 and d in z_dirs(s, hop - 1):
                back = hop - 1
                slot = (f + (n_fs - back if d == 0 else back)) % n_fs
                piece = s.ref(slot, s.rows)
                got(piece, z_recv.at[s.index, d, hop - 2], z_send.at[s.index], to)
                if s.paired:
                    rcopy(piece, piece, y_send.at[s.index], y_recv.at[s.index], to_pair).start()
            if hop <= half_ring and d in z_dirs(s, hop):
                back = hop - 1
                slot = (f + (n_fs - back if d == 0 else back)) % n_fs
                piece = s.ref(slot, s.rows)
                rcopy(piece, piece, z_send.at[s.index], z_recv.at[s.index, d, hop - 1], to).start()

    def y_done(name):
        s = streams[name]
        got(s.whole, y_recv.at[s.index], y_send.at[s.index], to_pair)

    def ag_rows(buf, slot, start, rows):
        return buf.at[slot, pl.ds(start, rows), :]

    def ag_a(ph, k, src, buf):
        rows = src(k * chunk, chunk)
        dst = ag_rows(buf, t, k * chunk, chunk)
        rcopy(rows, dst, ag_send.at[ph, k], ag_recv.at[ph, k, 0], to_right).start()
        rcopy(rows, dst, ag_send.at[ph, k], ag_recv.at[ph, k, 1], to_left).start()
        rcopy(rows, dst, agp_send.at[ph, k], agp_recv.at[ph, k], to_mate).start()

    def to_other_core(ph, k, piece):
        rcopy(piece, piece, agp_send.at[ph, k], agp_recv.at[ph, k], to_mate).start()

    def ag_b(ph, k, buf):
        for d, src_chip, lo, to in ((0, n_x - 1, 0, to_right), (1, 1, half, to_left)):
            slot = tp_of(src_chip)
            piece = ag_rows(buf, slot, k * chunk, chunk)
            got(piece, ag_recv.at[ph, k, d], ag_send.at[ph, k], to)
            part = ag_rows(buf, slot, k * chunk + lo, half)
            rcopy(part, part, ag_send.at[ph, k], ag_recv.at[ph, k, 2 + d], to).start()
            to_other_core(ph, k, piece)

    def ag_c(ph, k, buf):
        slot = tp_of(2)
        for d, lo in ((0, 0), (1, half)):
            part = ag_rows(buf, slot, k * chunk + lo, half)
            got(part, ag_recv.at[ph, k, 2 + d], ag_send.at[ph, k], to_right)
            to_other_core(ph, k, part)

    def ag_d(ph, k, buf):
        got(buf.at[pl.ds(0, n_x), pl.ds(k * chunk, chunk), :], agp_recv.at[ph, k], agp_send.at[ph, k], to_mate)

    def dest(w, rel, c):
        j = chip(rel) * CORES + c
        return jnp.concatenate([w[2 * j], w[2 * j + 1]], axis=1)

    ORDER = (2, 1, 3, 0)
    bufs = ((ps1, pr1, qs1, op1, fi1), (ps2, pr2, qs2, op2, fi2))

    def rs_a(ph, k, lhs, w):
        ps, pr = bufs[ph][:2]
        for rel in ORDER:
            right = dest(w, rel, 1 - core)

            def body(i, _):
                r = pl.multiple_of(i * ROWS, ROWS)
                ps[k, rel, pl.ds(r, ROWS), :] = jnp.dot(
                    lhs[pl.ds(k * chunk + r, ROWS), :], right, preferred_element_type=F32).astype(BF)
                return 0

            lax.fori_loop(0, chunk // ROWS, body, 0)
            rcopy(ps.at[k, rel], pr.at[k, rel], rp_send.at[ph, k], rp_recv.at[ph, k, rel], to_mate).start()

    def rs_b(ph, k, lhs, w):
        ps, pr, qs, op, fi = bufs[ph]
        for rel in ORDER:
            right = dest(w, rel, core)
            got(pr.at[k, rel], rp_recv.at[ph, k, rel], rp_send.at[ph, k], to_mate)

            def body(i, _):
                r = pl.multiple_of(i * ROWS, ROWS)
                qs[k, rel, pl.ds(r, ROWS), :] = (
                    jnp.dot(lhs[pl.ds(k * chunk + r, ROWS), :], right, preferred_element_type=F32)
                    + pr[k, rel, pl.ds(r, ROWS), :].astype(F32)).astype(BF)
                return 0

            lax.fori_loop(0, chunk // ROWS, body, 0)
            low, high = qs.at[k, rel, pl.ds(0, half), :], qs.at[k, rel, pl.ds(half, half), :]
            ss = rr_send.at[ph, k]
            if rel == 2:
                rcopy(low, op.at[0, k], ss, rr_recv.at[ph, k, 0], to_right).start()
                rcopy(high, op.at[1, k], ss, rr_recv.at[ph, k, 1], to_left).start()
            elif rel == 1:
                rcopy(high, fi.at[0, k, pl.ds(half, half), :], ss, rr_recv.at[ph, k, 2], to_right).start()
            elif rel == 3:
                rcopy(low, fi.at[1, k, pl.ds(0, half), :], ss, rr_recv.at[ph, k, 3], to_left).start()

    def rs_c(ph, k):
        ps, pr, qs, op, fi = bufs[ph]
        ss = rr_send.at[ph, k]
        for d, rel, lo, to in ((0, 1, 0, to_right), (1, 3, half, to_left)):
            got(op.at[d, k], rr_recv.at[ph, k, d], ss, to)
            rows = pl.ds(lo, half)
            qs[k, rel, rows, :] = (qs[k, rel, rows, :].astype(F32) + op[d, k].astype(F32)).astype(BF)
            rcopy(qs.at[k, rel, rows, :], fi.at[d, k, rows, :], ss, rr_recv.at[ph, k, 4 + d], to).start()

    def rs_d(ph, k, base, put):
        ps, pr, qs, op, fi = bufs[ph]
        ss = rr_send.at[ph, k]
        got(fi.at[0, k, pl.ds(half, half), :], rr_recv.at[ph, k, 2], ss, to_right)
        got(fi.at[1, k, pl.ds(0, half), :], rr_recv.at[ph, k, 3], ss, to_left)
        got(fi.at[0, k, pl.ds(0, half), :], rr_recv.at[ph, k, 4], ss, to_right)
        got(fi.at[1, k, pl.ds(half, half), :], rr_recv.at[ph, k, 5], ss, to_left)
        for r in range(0, chunk, ROWS):
            rows = pl.ds(r, ROWS)
            total = (qs[k, 0, rows, :].astype(F32) + fi[0, k, rows, :].astype(F32)
                     + fi[1, k, rows, :].astype(F32))
            put(k * chunk + r, (base(k * chunk + r).astype(F32) + total).astype(BF))

    def column(row):
        return jnp.broadcast_to(row, (row.shape[1], row.shape[1])).T

    def joined(buf, r):
        parts = [buf[j, pl.ds(r, ROWS), :] for j in range(n_tp)]
        squares = None
        for part in parts:
            wide = part.astype(F32)
            squares = wide * wide if squares is None else squares + wide * wide
        inv = lax.rsqrt(jnp.sum(squares, axis=1, keepdims=True) / feats + EPS)
        return jnp.concatenate(parts, axis=1), inv

    def gating(k):
        for r in range(0, chunk, ROWS):
            at = k * chunk + r
            lhs, inv = joined(xg, at)
            pre = jnp.dot(lhs, wuv[...], preferred_element_type=F32) * inv * suv_ref[...]
            act = jax.nn.gelu(pre)
            ub[pl.ds(at, ROWS), :] = act[:, :u_w]
            turned = act[:, u_w:].T
            vt[:, pl.ds(at, ROWS)] = turned
            st_own[k, :, pl.ds(r, ROWS)] = jnp.concatenate(
                [jnp.sum(turned, axis=0, keepdims=True), jnp.sum(turned * turned, axis=0, keepdims=True),
                 jnp.zeros((6, ROWS), F32)], axis=0)
        rcopy(st_own.at[k], st_p.at[k], st_send.at[k], st_recv.at[k, 3], to_mate).start()

    def stats(k):
        got(st_p.at[k], st_recv.at[k, 3], st_send.at[k], to_mate)
        st_c[k] = st_own[k] + st_p[k]
        for n, to in enumerate((to_right, to_left, to_opp)):
            rcopy(st_c.at[k], st_x.at[n, k], st_send.at[k], st_recv.at[k, n], to).start()

    def mixing(k):
        for n in range(3):
            got(st_x.at[n, k], st_recv.at[k, n], st_send.at[k], to_mate)
        total = st_c[k] + st_x[0, k] + st_x[1, k] + st_x[2, k]
        mean = total[0:1] / gm_w
        square = total[1:2] / gm_w
        scale = lax.rsqrt(square - mean * mean + EPS)
        gain = column(mg_ref[...])[:, 0:1]
        for b in range(0, chunk, block):
            at = k * chunk + b
            v_norm = ((vt[:, pl.ds(at, block)] - mean[:, b:b + block]) * scale[:, b:b + block] * gain).astype(BF)
            mixed = lax.dot_general(mask[...], v_norm, (((1,), (1,)), ((), ())), preferred_element_type=F32)
            gated[pl.ds(at, block), :] = (ub[pl.ds(at, block), :] * (mixed + bias[...])).astype(BF)

    def ff_up(k):
        for r in range(0, chunk, ROWS):
            at = k * chunk + r
            lhs, inv = joined(rg, at)
            for n in range(0, h_w, 256):
                cols = pl.ds(n, 256)
                acc = jnp.dot(lhs, wup[:, n:n + 256], preferred_element_type=F32)
                acc = jnp.maximum(acc * inv * sup_ref[:, n:n + 256], 0.0)
                hid[pl.ds(at, ROWS), cols] = (acc * acc).astype(BF)

    def rounded(w):
        return w.astype(BF).astype(F32)

    own = pl.ds(pl.multiple_of(f * k_fs, k_fs), k_fs)

    tokens_at = lambda r, n: x_ref.at[pl.ds(r, n), :]
    res_at = lambda r, n: ag_rows(rg, t, r, n)
    for k in range(CHUNKS):
        ag_a(0, k, tokens_at, xg)

    g1 = column(g1_ref[pl.ds(f, 1), :])
    wuv[own, :] = (jnp.concatenate([rounded(wu_ref[...]) * g1, rounded(wv_ref[...]) * g1], axis=1)).astype(BF)
    z_hop("uv", 1)
    g2 = column(g2_ref[pl.ds(f, 1), :])[:, 0:1]
    wup[own, :] = (rounded(wup_ref[...]) * g2).astype(BF)
    A1 = ("uv", "upy", "out")
    B1 = ("upb", "dny", "dnb")
    z_hop("upy", 1)
    wout[f] = (rounded(wo_ref[...]) * so_ref[...]).astype(BF)
    z_hop("out", 1)
    xg[t] = x_ref[...]
    wdn[f] = (rounded(wdn_ref[...]) * sdn_ref[...]).astype(BF)
    low = lax.broadcasted_iota(jnp.int32, (block, block), 0) >= lax.broadcasted_iota(jnp.int32, (block, block), 1)
    grp_at = t * u_w // (gm_w // sw_ref.shape[0])
    mask[...] = jnp.where(low, sw_ref[grp_at], 0.0).astype(BF)
    bias[...] = column(sb_ref[pl.ds(grp_at, 1), :])

    def z_round(names, hop):
        for name in names:
            z_hop(name, hop)

    z_round(A1, 2)
    z_round(A1, 3)
    ag_b(0, 0, xg)
    z_round(A1, 4)
    ag_b(0, 1, xg)
    z_round(A1, 5)
    ag_c(0, 0, xg)
    z_round(A1, 6)
    ag_c(0, 1, xg)
    z_round(A1, 7)
    ag_d(0, 0, xg)
    ag_d(0, 1, xg)
    z_round(A1, 8)
    z_round(B1, 1)
    z_round(A1, 9)

    gating(0)
    gating(1)
    stats(0)
    stats(1)
    z_round(B1, 2)
    mixing(0)
    rs_a(0, 0, gated, wout)
    mixing(1)
    rs_a(0, 1, gated, wout)
    rs_b(0, 0, gated, wout)
    rs_b(0, 1, gated, wout)
    z_round(B1, 3)
    rs_c(0, 0)
    z_round(B1, 4)
    rs_c(0, 1)

    def base1(r):
        return x_ref[pl.ds(r, ROWS), :]

    def put1(r, v):
        rg[t, pl.ds(r, ROWS), :] = v

    rs_d(0, 0, base1, put1)
    ag_a(1, 0, res_at, rg)
    z_round(B1, 5)
    rs_d(0, 1, base1, put1)
    ag_a(1, 1, res_at, rg)
    z_round(B1, 6)
    ag_b(1, 0, rg)
    z_round(B1, 7)
    ag_b(1, 1, rg)
    z_round(B1, 8)
    ag_c(1, 0, rg)
    z_round(B1, 9)
    ag_c(1, 1, rg)
    y_done("upy")
    ag_d(1, 0, rg)
    ff_up(0)
    y_done("dny")
    rs_a(1, 0, hid, wdn)
    ag_d(1, 1, rg)
    rs_b(1, 0, hid, wdn)
    ff_up(1)
    rs_c(1, 0)
    rs_a(1, 1, hid, wdn)
    rs_b(1, 1, hid, wdn)

    def base2(r):
        return rg[t, pl.ds(r, ROWS), :]

    def put2(r, v):
        out_ref[pl.ds(r, ROWS), :] = v

    rs_d(1, 0, base2, put2)
    rs_c(1, 1)
    rs_d(1, 1, base2, put2)

    for s in streams.values():
        sent(s.whole, z_send.at[s.index], z_recv.at[s.index, 0, 0], to_up)
        if s.paired:
            sent(s.whole, y_send.at[s.index], y_recv.at[s.index], to_pair)
    for ph, buf in ((0, xg), (1, rg)):
        ps, pr, qs, op, fi = bufs[ph]
        for k in range(CHUNKS):
            rows = pl.ds(k * chunk, chunk)
            sent(buf.at[pl.ds(0, 3), rows, :], ag_send.at[ph, k], ag_recv.at[ph, k, 0], to_right)
            sent(buf.at[pl.ds(0, n_x), rows, :], agp_send.at[ph, k], agp_recv.at[ph, k], to_mate)
            sent(ps.at[k], rp_send.at[ph, k], rp_recv.at[ph, k, 0], to_mate)
            sent(qs.at[k, pl.ds(0, 3)], rr_send.at[ph, k], rr_recv.at[ph, k, 0], to_right)
    for k in range(CHUNKS):
        sent(st_x.at[pl.ds(0, 4), k], st_send.at[k], st_recv.at[k, 0], to_mate)


def per_device(dims, tokens, norm1_gain, weight_u, weight_v, scale_u, scale_v, mix_gain, spatial_weight,
               spatial_bias, weight_out, scale_out, norm2_gain, weight_up, scale_up, weight_down, scale_down):
    n_fs, n_tp = dims["fs"], dims["tp"]
    rows, width = tokens.shape
    feats = width * n_tp
    u_w, h_w = weight_u.shape[1], weight_up.shape[1]
    o_w, d_w = weight_out.shape[1], weight_down.shape[1]
    chunk = rows // CHUNKS
    block = spatial_weight.shape[1]
    n_x = n_tp // CORES
    if n_x != 4 or width != 2 * o_w or width != 2 * d_w:
        raise ValueError("unsupported mesh")
    args = (
        tokens, norm1_gain.reshape(n_fs, -1), weight_u, weight_v,
        jnp.concatenate([scale_u, scale_v]).reshape(1, -1), mix_gain.reshape(1, -1), spatial_weight, spatial_bias,
        weight_out, scale_out.reshape(1, -1), norm2_gain.reshape(n_fs, -1), weight_up, scale_up.reshape(1, -1),
        weight_down, scale_down.reshape(1, -1),
    )
    rs = [
        pltpu.VMEM((CHUNKS, n_x, chunk, width), BF),
        pltpu.VMEM((CHUNKS, n_x, chunk, width), BF),
        pltpu.VMEM((CHUNKS, n_x, chunk, width), BF),
        pltpu.VMEM((2, CHUNKS, chunk // 2, width), BF),
        pltpu.VMEM((2, CHUNKS, chunk, width), BF),
    ]
    dma = pltpu.SemaphoreType.DMA
    n_streams = 6
    scratch = [
        pltpu.VMEM((feats, 2 * u_w), BF),
        pltpu.VMEM((n_fs, u_w, o_w), BF),
        pltpu.VMEM((feats, h_w), BF),
        pltpu.VMEM((n_fs, h_w, d_w), BF),
        pltpu.VMEM((n_tp, rows, width), BF),
        pltpu.VMEM((n_tp, rows, width), BF),
        pltpu.VMEM((rows, u_w), F32),
        pltpu.VMEM((u_w, rows), F32),
        pltpu.VMEM((CHUNKS, 8, chunk), F32),
        pltpu.VMEM((CHUNKS, 8, chunk), F32),
        pltpu.VMEM((CHUNKS, 8, chunk), F32),
        pltpu.VMEM((4, CHUNKS, 8, chunk), F32),
        pltpu.VMEM((rows, u_w), BF),
        pltpu.VMEM((rows, h_w), BF),
        *rs, *rs,
        pltpu.VMEM((block, block), BF),
        pltpu.VMEM((block, block), F32),
        dma((n_streams, 2, n_fs // 2)), dma((n_streams,)), dma((n_streams,)), dma((n_streams,)),
        dma((2, CHUNKS, 4)), dma((2, CHUNKS)), dma((2, CHUNKS)), dma((2, CHUNKS)),
        dma((2, CHUNKS, n_x)), dma((2, CHUNKS)), dma((2, CHUNKS, 6)), dma((2, CHUNKS)),
        dma((CHUNKS, 4)), dma((CHUNKS,)),
    ]
    vmem = pl.BlockSpec(memory_space=pltpu.VMEM)
    return pl.pallas_call(
        functools.partial(kernel, dims),
        out_shape=jax.ShapeDtypeStruct(tokens.shape, tokens.dtype),
        in_specs=[vmem] * len(args),
        out_specs=vmem,
        scratch_shapes=scratch,
        name="layer",
        compiler_params=pltpu.CompilerParams(
            collective_id=0, has_side_effects=True, vmem_limit_bytes=64 * 1000 * 1000),
    )(*args)


def solution(mesh):
    placed = (
        P(("grp", "fs"), "tp"), P(), P("fs", "tp"), P("fs", "tp"), P("tp"), P("tp"), P("tp"), P(), P(),
        P("tp", "fs"), P("fs"), P(), P("fs", "tp"), P("tp"), P("tp", "fs"), P("fs"),
    )
    return jax.shard_map(
        functools.partial(per_device, dict(mesh.shape)), mesh=mesh, in_specs=placed,
        out_specs=P(("grp", "fs"), "tp"), check_vma=False)
```

time: 442 us -> 141 us (0.32)
  blocking collectives: 195 us -> 0 us
  waiting for transfers between devices: 170 us -> 0 us
  Pallas kernels: 0 us -> 138 us
  matrix products: 28.1 us -> 0 us
  starting transfers between devices: 16.6 us -> 0 us
  between operations: 13.4 us -> 0.01 us
  other arithmetic: 10.7 us -> 0.57 us
  local copies, waits for them, and re-layouts: 7.6 us -> 2.54 us
    all_gather x5 -> x0, waiting for transfers between devices: 164 us -> none  [the longest x1 51.7 us: per_device(): lax.all_gather(tokens, 'tp', axis=1, tiled=True).astype(jnp.float32)]
    all_to_all x4 -> x0, blocking collectives: 144 us -> none  [the longest x2 109 us: sent_and_summed(): lax.all_to_all(parts, axis, split_axis=0, concat_axis=0, tiled=True)]
    pallas_call x0 -> x1, Pallas kernels: none -> 138 us  [per_device(): pl.pallas_call(functools.partial(kernel, dims), out_shape=jax.ShapeDtypeS...]
    all_gather x1 -> x0, blocking collectives: 50.6 us -> none  [rows_first(): lax.all_gather(both, axis, axis=0, tiled=True)]
    dot_general x4 -> x0, matrix products: 28.1 us -> none  [the longest x1 14.7 us: per_device(): lax.dot_general(columns, hidden, (((0,), (1,)), ((), ())), preferred_elem...]
    all_to_all x2 -> x0, starting transfers between devices: 16.3 us -> none  [from_everyone(): lax.all_to_all(jnp.broadcast_to(shard[None], (peers, *shard.shape)), axis...]
    convert_element_type x7 -> x0, other arithmetic: 6.54 us -> none  [the longest x1 1.79 us: per_device(): down_rounded = weight_down.astype(jnp.bfloat16)]
    reshape x2 -> x0, local copies, waits for them, and re-layouts: 4.94 us -> none  [split_up(): shard.reshape(*dims[:dim], peers, dims[dim] // peers, *dims[dim + 1:])]
  transfers between devices with their start and end apart: 7 -> 0, of which waited for: 5 -> 0; matrix products, arithmetic and copies ran while one was open for 6% -> 0% of each run, Pallas kernels for 0% -> 0%
where the time goes in v1:
time: 141 us
  Pallas kernels  138 us (98%)
  local copies, waits for them, and re-layouts  2.54 us (2%)
    pallas_call x1, Pallas kernels, per_device(): pl.pallas_call(functools.partial(kernel, dims), out_shape=jax.ShapeDtypeS...  138 us

profile of v1, /device:TPU:33, one launch (start us, length us, event | category | flops | bytes accessed | tf_op | source)
XLA Modules:
  0.0 141.2 jit_solution(12128121380816013931)
XLA Ops:
  0.0 0.0 copy-start
  0.0 0.0 copy-start.1
  0.0 0.7 copy-done
  0.7 0.0 copy-done.1
  0.7 0.6 pad_maximum_fusion
  1.2 138.0 %layer.1 = bf16[1024,256]{1,0:T(8,128)(2,1)} custom-call(bf16[1024,256]{1,0:T(8,128)(2,1)} %x_ref.1, f32[16,128]{1,0:T(8,128)} %bitcast.7, f32[128,128]{1,0:T(8,128)} %wu_ref.1, f32[128,128]{1,0:T(8,128)} %wv_ref.1, f32[1,256]{1,0:T(1,128)} %bitcast.10, f32[1,128]{1,0:T(1,128)} %bitcast.11, f32[4,128,128]{2,1,0:T(8,128)} %sw_ref.1, f32[4,128]{1,0:T(4,128)} %sb_ref.1, ...), custom_call_target="tpu_custom_call" | custom-call | tf_op jit(solution)/shard_map/layer/pallas_call | solution.py:467
  139.3 1.9 %copy.18 = bf16[1024,256]{1,0:T(8,128)(2,1)} copy(bf16[1024,256]{1,0:T(8,128)(2,1)} %layer.1) | data formatting | bytes 1048576
Async XLA Ops:
  0.0 0.7 copy-start
  0.0 0.7 copy-start.1

commit v2 on v1

v2 whole, which is shorter than its diff:
```python
import functools

import jax
import jax.numpy as jnp
from jax import lax
from jax.experimental import pallas as pl
from jax.experimental.pallas import tpu as pltpu
from jax.sharding import PartitionSpec as P

BF = jnp.bfloat16
F32 = jnp.float32
MESH = pl.DeviceIdType.MESH
EPS = 1e-06
CORES = 2
CHUNKS = 2
ROWS = 256


class Stream:
    def __init__(self, name, ref, rows, whole, paired):
        self.name, self.ref, self.rows, self.whole, self.paired = name, ref, rows, whole, paired


def kernel(
    dims,
    x_ref, g1_ref, wu_ref, wv_ref, su_ref, sv_ref, mg_ref, sw_ref, sb_ref, wo_ref, so_ref,
    g2_ref, wup_ref, sup_ref, wdn_ref, sdn_ref,
    out_ref,
    wuv, wout, wup, wdn, xg, rg, ub, vt, st_own, st_p, st_c, st_x, gated, hid,
    ps1, pr1, qs1, op1, fi1, ps2, pr2, qs2, op2, fi2, mask, bias, total_e,
    z_recv, z_send, y_recv, y_send, ag_recv, ag_send, agp_recv, agp_send,
    rp_recv, rp_send, rr_recv, rr_send, st_recv, st_send,
):
    n_fs, n_tp = dims["fs"], dims["tp"]
    n_x = n_tp // CORES
    half_ring = n_fs // 2
    total_rows, width = x_ref.shape
    feats = width * n_tp
    u_w = wu_ref.shape[1]
    k_fs = wu_ref.shape[0]
    h_w = wup_ref.shape[1]
    gm_w = u_w * n_tp
    chunk = total_rows // CHUNKS
    half = chunk // 2
    block = sw_ref.shape[1]
    pair = dims["grp"] % 2 == 0

    g = lax.axis_index("grp")
    f = lax.axis_index("fs")
    t = lax.axis_index("tp")
    cx = t // CORES
    core = t % CORES
    par = g % 2

    def chip(d):
        return (cx + d) % n_x

    def tp_of(d):
        return chip(d) * CORES + core

    to_right, to_left, to_opp = {"tp": tp_of(1)}, {"tp": tp_of(n_x - 1)}, {"tp": tp_of(2)}
    to_mate = {"tp": cx * CORES + 1 - core}
    to_up, to_down = {"fs": (f + 1) % n_fs}, {"fs": (f + n_fs - 1) % n_fs}
    to_pair = {"grp": g + 1 - 2 * par}

    to_up2, to_down2 = {"fs": (f + 2) % n_fs}, {"fs": (f + n_fs - 2) % n_fs}
    neighbours = [to_right, to_left, to_opp, to_mate, to_up, to_down, to_up2, to_down2]
    if pair:
        neighbours.append(to_pair)
    barrier = pltpu.get_barrier_semaphore()
    for n in neighbours:
        pl.semaphore_signal(barrier, inc=1, device_id=n, device_id_type=MESH)
    pl.semaphore_wait(barrier, len(neighbours))

    def rcopy(src, dst, ss, rs, dev):
        return pltpu.make_async_remote_copy(
            src_ref=src, dst_ref=dst, send_sem=ss, recv_sem=rs, device_id=dev, device_id_type=MESH)

    def got(ref, sem, spare, dev):
        rcopy(ref, ref, spare, sem, dev).wait_recv()

    def sent(ref, sem, spare, dev):
        rcopy(ref, ref, sem, spare, dev).wait_send()

    def rows_2d(ref, start):
        def at(slot, rows):
            return ref.at[pl.ds(pl.multiple_of(slot * k_fs + start, 16), rows), :]
        return at

    def rows_3d(ref, start):
        def at(slot, rows):
            return ref.at[slot, pl.ds(pl.multiple_of(start, 16), rows), :]
        return at

    def whole_2d(ref, rows):
        return ref.at[pl.ds(0, (n_fs - 1) * rows), :]

    def whole_3d(ref, rows):
        return ref.at[pl.ds(0, n_fs - 1), pl.ds(0, rows), :]

    def make(name, ref, three, first, own_rows, swap):
        def at(r, start):
            return (rows_3d if three else rows_2d)(r, first + start)

        whole = whole_3d if three else whole_2d
        result = []
        if pair and swap:
            shared = own_rows - 2 * swap
            result.append(Stream(name + "y", at(ref, par * (own_rows - swap)), swap, whole(ref, swap), True))
            if shared:
                result.append(Stream(name + "b", at(ref, swap), shared, whole(ref, shared), False))
        else:
            result.append(Stream(name + "y", at(ref, 0), own_rows, whole(ref, own_rows), False))
        return result

    streams = {}
    dn_half = k_fs // 2
    for s in (make("uv", wuv, False, 0, k_fs, k_fs // 2) + make("out", wout, True, 0, u_w, u_w // 2)
              + make("up", wup, False, 0, k_fs, 32) + make("e", wdn, False, 0, dn_half, 32)
              + make("f", wdn, False, dn_half, dn_half, 16)):
        s.index = len(streams)
        streams[s.name] = s

    def z_dirs(s, hop):
        return (0, 1) if hop < half_ring else (s.index % 2,)

    def z_hop(name, hop):
        s = streams[name]
        for d in (0, 1):
            to = to_up if d == 0 else to_down
            if hop > 1 and d in z_dirs(s, hop - 1):
                back = hop - 1
                slot = (f + (n_fs - back if d == 0 else back)) % n_fs
                piece = s.ref(slot, s.rows)
                got(piece, z_recv.at[s.index, d, hop - 2], z_send.at[s.index], to)
                if s.paired:
                    rcopy(piece, piece, y_send.at[s.index], y_recv.at[s.index], to_pair).start()
            if hop <= half_ring and d in z_dirs(s, hop):
                back = hop - 1
                slot = (f + (n_fs - back if d == 0 else back)) % n_fs
                piece = s.ref(slot, s.rows)
                rcopy(piece, piece, z_send.at[s.index], z_recv.at[s.index, d, hop - 1], to).start()

    FAST = ("uvy", "outy")
    stages = half_ring // 2

    def slot_at(d, back):
        return (f + (n_fs - back if d == 0 else back)) % n_fs

    def fast_piece(s, d, back):
        return s.ref(slot_at(d, back), s.rows)

    def fast_got(s, d, back):
        got(fast_piece(s, d, back), z_recv.at[s.index, d, back - 1], z_send.at[s.index], to_up)

    def to_partner(s, piece):
        if s.paired:
            rcopy(piece, piece, y_send.at[s.index], y_recv.at[s.index], to_pair).start()

    def fast(stage):
        even = 2 * (stage - 1)
        for name in FAST:
            s = streams[name]
            for d in (0, 1):
                one, two = (to_up, to_up2) if d == 0 else (to_down, to_down2)
                if stage > 1 and d in z_dirs(s, even):
                    fast_got(s, d, even)
                    to_partner(s, fast_piece(s, d, even))
                if stage <= stages:
                    piece = fast_piece(s, d, even)
                    for step, to in ((2, two), (1, one)):
                        if d in z_dirs(s, even + step):
                            rcopy(piece, piece, z_send.at[s.index], z_recv.at[s.index, d, even + step - 1], to).start()
        if stage > 1:
            for name in FAST:
                s = streams[name]
                for d in (0, 1):
                    fast_got(s, d, even - 1)
                    to_partner(s, fast_piece(s, d, even - 1))

    def y_done(name):
        s = streams[name]
        if not s.paired:
            return
        got(s.whole, y_recv.at[s.index], y_send.at[s.index], to_pair)

    def ag_rows(buf, slot, start, rows):
        return buf.at[slot, pl.ds(start, rows), :]

    def ag_a(ph, k, src, buf):
        for n, to, lo in ((0, to_right, 0), (1, to_right, half), (2, to_left, half), (3, to_left, 0)):
            at = k * chunk + lo
            rcopy(src(at, half), ag_rows(buf, t, at, half), ag_send.at[ph, k], ag_recv.at[ph, k, n], to).start()
        at = k * chunk
        rcopy(src(at, chunk), ag_rows(buf, t, at, chunk), agp_send.at[ph, k], agp_recv.at[ph, k], to_mate).start()

    def to_other_core(ph, k, piece):
        rcopy(piece, piece, agp_send.at[ph, k], agp_recv.at[ph, k], to_mate).start()

    def ag_b(ph, k, buf):
        for n, src_chip, lo, to in ((0, n_x - 1, 0, to_right), (2, 1, half, to_left)):
            part = ag_rows(buf, tp_of(src_chip), k * chunk + lo, half)
            got(part, ag_recv.at[ph, k, n], ag_send.at[ph, k], to)
            rcopy(part, part, ag_send.at[ph, k], ag_recv.at[ph, k, 4 + n // 2], to).start()

    def ag_c(ph, k, buf):
        for n, src_chip, lo, to in ((1, n_x - 1, half, to_right), (3, 1, 0, to_left)):
            part = ag_rows(buf, tp_of(src_chip), k * chunk + lo, half)
            got(part, ag_recv.at[ph, k, n], ag_send.at[ph, k], to)
            to_other_core(ph, k, ag_rows(buf, tp_of(src_chip), k * chunk, chunk))

    def ag_e(ph, k, buf):
        for n, lo in ((4, 0), (5, half)):
            part = ag_rows(buf, tp_of(2), k * chunk + lo, half)
            got(part, ag_recv.at[ph, k, n], ag_send.at[ph, k], to_right)
            to_other_core(ph, k, part)

    def ag_d(ph, k, buf):
        got(buf.at[pl.ds(0, n_x), pl.ds(k * chunk, chunk), :], agp_recv.at[ph, k], agp_send.at[ph, k], to_mate)

    bufs = ((ps1, pr1, qs1, op1, fi1), (ps2, pr2, qs2, op2, fi2))

    def products(ph, u, c):
        k, e = u % CHUNKS, u // CHUNKS
        if ph == 0:
            left = gated[pl.ds(k * chunk, chunk), :]
            for rel in (2, 1, 3, 0):
                j = chip(rel) * CORES + c
                right = jnp.concatenate([wout[2 * j], wout[2 * j + 1]], axis=1)
                yield ((rel, jnp.dot(left, right, preferred_element_type=F32)),)
        else:
            left = hid[pl.ds(k * chunk, chunk), :]
            for rels in ((2, 1), (3, 0)):
                parts = []
                for rel in rels:
                    j = chip(rel) * CORES + c
                    for shard in (2 * j, 2 * j + 1):
                        at = pl.multiple_of(shard * k_fs + e * dn_half, dn_half)
                        parts.append(wdn[pl.ds(at, dn_half), :])
                both = lax.dot_general(left, jnp.concatenate(parts, axis=0), (((1,), (1,)), ((), ())),
                                       preferred_element_type=F32)
                yield ((rels[0], both[:, :k_fs]), (rels[1], both[:, k_fs:]))

    def rs_a(ph, u):
        ps, pr = bufs[ph][:2]
        for some in products(ph, u, 1 - core):
            for rel, value in some:
                ps[u, rel] = value.astype(BF)
                rcopy(ps.at[u, rel], pr.at[u, rel], rp_send.at[ph, u], rp_recv.at[ph, u, rel], to_mate).start()

    def rs_b(ph, u):
        ps, pr, qs, op, fi = bufs[ph]
        ss = rr_send.at[ph, u]
        for some in products(ph, u, core):
            for rel, value in some:
                got(pr.at[u, rel], rp_recv.at[ph, u, rel], rp_send.at[ph, u], to_mate)
                qs[u, rel] = (value + pr[u, rel].astype(F32)).astype(BF)
                low, high = qs.at[u, rel, pl.ds(0, half), :], qs.at[u, rel, pl.ds(half, half), :]
                if rel == 2:
                    rcopy(low, op.at[0, u], ss, rr_recv.at[ph, u, 0], to_right).start()
                    rcopy(high, op.at[1, u], ss, rr_recv.at[ph, u, 1], to_left).start()
                elif rel == 1:
                    rcopy(high, fi.at[0, u, pl.ds(half, half), :], ss, rr_recv.at[ph, u, 2], to_right).start()
                elif rel == 3:
                    rcopy(low, fi.at[1, u, pl.ds(0, half), :], ss, rr_recv.at[ph, u, 3], to_left).start()

    def rs_c(ph, u):
        ps, pr, qs, op, fi = bufs[ph]
        ss = rr_send.at[ph, u]
        for d, rel, lo, to in ((0, 1, 0, to_right), (1, 3, half, to_left)):
            got(op.at[d, u], rr_recv.at[ph, u, d], ss, to)
            rows = pl.ds(lo, half)
            qs[u, rel, rows, :] = (qs[u, rel, rows, :].astype(F32) + op[d, u].astype(F32)).astype(BF)
            rcopy(qs.at[u, rel, rows, :], fi.at[d, u, rows, :], ss, rr_recv.at[ph, u, 4 + d], to).start()

    def rs_d(ph, u, put):
        ps, pr, qs, op, fi = bufs[ph]
        ss = rr_send.at[ph, u]
        got(fi.at[0, u, pl.ds(half, half), :], rr_recv.at[ph, u, 2], ss, to_right)
        got(fi.at[1, u, pl.ds(0, half), :], rr_recv.at[ph, u, 3], ss, to_left)
        got(fi.at[0, u, pl.ds(0, half), :], rr_recv.at[ph, u, 4], ss, to_right)
        got(fi.at[1, u, pl.ds(half, half), :], rr_recv.at[ph, u, 5], ss, to_left)
        for r in range(0, chunk, ROWS):
            rows = pl.ds(r, ROWS)
            put((u % CHUNKS) * chunk + r, qs[u, 0, rows, :].astype(F32) + fi[0, u, rows, :].astype(F32)
                + fi[1, u, rows, :].astype(F32))

    def column(row):
        return jnp.broadcast_to(row, (row.shape[1], row.shape[1])).T

    def joined(buf, r):
        parts = [buf[j, pl.ds(r, ROWS), :] for j in range(n_tp)]
        squares = None
        for part in parts:
            wide = part.astype(F32)
            squares = wide * wide if squares is None else squares + wide * wide
        inv = lax.rsqrt(jnp.sum(squares, axis=1, keepdims=True) / feats + EPS)
        return jnp.concatenate(parts, axis=1), inv

    def gating(k):
        scale_uv = jnp.concatenate([su_ref[...], sv_ref[...]], axis=1)
        for r in range(0, chunk, ROWS):
            at = k * chunk + r
            lhs, inv = joined(xg, at)
            pre = jnp.dot(lhs, wuv[...], preferred_element_type=F32) * inv * scale_uv
            act = jax.nn.gelu(pre)
            ub[pl.ds(at, ROWS), :] = act[:, :u_w]
            turned = act[:, u_w:].T
            vt[:, pl.ds(at, ROWS)] = turned
            st_own[k, :, pl.ds(r, ROWS)] = jnp.concatenate(
                [jnp.sum(turned, axis=0, keepdims=True), jnp.sum(turned * turned, axis=0, keepdims=True),
                 jnp.zeros((6, ROWS), F32)], axis=0)
        rcopy(st_own.at[k], st_p.at[k], st_send.at[k], st_recv.at[k, 3], to_mate).start()

    def stats(k):
        got(st_p.at[k], st_recv.at[k, 3], st_send.at[k], to_mate)
        st_c[k] = st_own[k] + st_p[k]
        for n, to in enumerate((to_right, to_left, to_opp)):
            rcopy(st_c.at[k], st_x.at[n, k], st_send.at[k], st_recv.at[k, n], to).start()

    def mixing(k):
        for n in range(3):
            got(st_x.at[n, k], st_recv.at[k, n], st_send.at[k], to_mate)
        total = st_c[k] + st_x[0, k] + st_x[1, k] + st_x[2, k]
        mean = total[0:1] / gm_w
        square = total[1:2] / gm_w
        scale = lax.rsqrt(square - mean * mean + EPS)
        gain = column(mg_ref[...])[:, 0:1]
        for b in range(0, chunk, block):
            at = k * chunk + b
            v_norm = ((vt[:, pl.ds(at, block)] - mean[:, b:b + block]) * scale[:, b:b + block] * gain).astype(BF)
            mixed = lax.dot_general(mask[...], v_norm, (((1,), (1,)), ((), ())), preferred_element_type=F32)
            gated[pl.ds(at, block), :] = (ub[pl.ds(at, block), :] * (mixed + bias[...])).astype(BF)

    def ff_up(k):
        for r in range(0, chunk, ROWS):
            at = k * chunk + r
            lhs, inv = joined(rg, at)
            for n in range(0, h_w, 256):
                cols = pl.ds(n, 256)
                acc = jnp.dot(lhs, wup[:, n:n + 256], preferred_element_type=F32)
                acc = jnp.maximum(acc * inv * sup_ref[:, n:n + 256], 0.0)
                hid[pl.ds(at, ROWS), cols] = (acc * acc).astype(BF)

    def rounded(w):
        return w.astype(BF).astype(F32)

    own = pl.ds(pl.multiple_of(f * k_fs, k_fs), k_fs)

    tokens_at = lambda r, n: x_ref.at[pl.ds(r, n), :]
    res_at = lambda r, n: ag_rows(rg, t, r, n)
    for k in range(CHUNKS):
        ag_a(0, k, tokens_at, xg)

    g1 = column(g1_ref[pl.ds(f, 1), :])
    wuv[own, :] = (jnp.concatenate([rounded(wu_ref[...]) * g1, rounded(wv_ref[...]) * g1], axis=1)).astype(BF)
    wout[f] = (rounded(wo_ref[...]) * so_ref[...]).astype(BF)
    fast(1)
    g2 = column(g2_ref[pl.ds(f, 1), :])[:, 0:1]
    wup[own, :] = (rounded(wup_ref[...]) * g2).astype(BF)
    z_hop("upb", 1)
    wdn[own, :] = (rounded(wdn_ref[...]) * sdn_ref[...]).T.astype(BF)
    xg[t] = x_ref[...]
    low = lax.broadcasted_iota(jnp.int32, (block, block), 0) >= lax.broadcasted_iota(jnp.int32, (block, block), 1)
    grp_at = t * u_w // (gm_w // sw_ref.shape[0])
    mask[...] = jnp.where(low, sw_ref[grp_at], 0.0).astype(BF)
    bias[...] = column(sb_ref[pl.ds(grp_at, 1), :])

    def z_round(*pairs):
        for name, hop in pairs:
            z_hop(name, hop)

    fast(2)
    z_hop("upb", 2)
    ag_b(0, 0, xg)
    fast(3)
    z_hop("upb", 3)
    ag_b(0, 1, xg)
    ag_c(0, 0, xg)
    fast(4)
    z_hop("upb", 4)
    ag_c(0, 1, xg)
    ag_e(0, 0, xg)
    fast(5)
    z_round(("upb", 5), ("upy", 1))
    ag_e(0, 1, xg)
    y_done("uvy")
    ag_d(0, 0, xg)
    gating(0)
    ag_d(0, 1, xg)
    gating(1)
    stats(0)
    stats(1)
    z_round(("upb", 6), ("upy", 2))
    y_done("outy")
    mixing(0)
    rs_a(0, 0)
    mixing(1)
    rs_b(0, 0)
    rs_a(0, 1)
    z_round(("upb", 7), ("upy", 3), ("ey", 1))
    rs_c(0, 0)
    rs_b(0, 1)
    z_round(("upb", 8), ("upy", 4), ("ey", 2))

    def put1(r, v):
        rg[t, pl.ds(r, ROWS), :] = (x_ref[pl.ds(r, ROWS), :].astype(F32) + v).astype(BF)

    rs_d(0, 0, put1)
    ag_a(1, 0, res_at, rg)
    rs_c(0, 1)
    z_round(("upb", 9), ("upy", 5), ("ey", 3), ("fy", 1), ("fb", 1))
    rs_d(0, 1, put1)
    ag_b(1, 0, rg)
    ag_a(1, 1, res_at, rg)
    z_round(("upy", 6), ("ey", 4), ("fy", 2), ("fb", 2))
    ag_c(1, 0, rg)
    z_round(("upy", 7), ("ey", 5), ("fy", 3), ("fb", 3))
    ag_e(1, 0, rg)
    ag_b(1, 1, rg)
    z_round(("upy", 8), ("ey", 6), ("fy", 4), ("fb", 4))
    ag_c(1, 1, rg)
    ag_d(1, 0, rg)
    z_round(("upy", 9), ("ey", 7), ("fy", 5), ("fb", 5))
    ag_e(1, 1, rg)
    y_done("upy")
    ff_up(0)
    z_round(("ey", 8), ("fy", 6), ("fb", 6))
    ag_d(1, 1, rg)
    ff_up(1)
    z_round(("ey", 9), ("fy", 7), ("fb", 7))
    y_done("ey")
    rs_a(1, 0)
    rs_b(1, 0)
    z_round(("fy", 8), ("fb", 8))
    rs_a(1, 1)
    rs_c(1, 0)
    rs_b(1, 1)
    z_round(("fy", 9), ("fb", 9))
    rs_c(1, 1)
    y_done("fy")
    rs_a(1, 2)
    rs_b(1, 2)

    def put_e(r, v):
        total_e[pl.ds(r, ROWS), :] = v

    def put2(r, v):
        rows = pl.ds(r, ROWS)
        first, h = total_e[rows, :], dn_half
        total = jnp.concatenate([first[:, :h], v[:, :h], first[:, h:], v[:, h:]], axis=1)
        out_ref[rows, :] = (rg[t, rows, :].astype(F32) + total).astype(BF)

    rs_a(1, 3)
    rs_d(1, 0, put_e)
    rs_c(1, 2)
    rs_b(1, 3)
    rs_d(1, 1, put_e)
    rs_c(1, 3)
    rs_d(1, 2, put2)
    rs_d(1, 3, put2)

    for s in streams.values():
        sent(s.whole, z_send.at[s.index], z_recv.at[s.index, 0, 0], to_up)
        if s.paired:
            sent(s.whole, y_send.at[s.index], y_recv.at[s.index], to_pair)
    for ph, buf in ((0, xg), (1, rg)):
        ps, pr, qs, op, fi = bufs[ph]
        for k in range(CHUNKS):
            rows = pl.ds(k * chunk, chunk)
            sent(buf.at[pl.ds(0, 3), rows, :], ag_send.at[ph, k], ag_recv.at[ph, k, 0], to_right)
            sent(buf.at[pl.ds(0, n_x), rows, :], agp_send.at[ph, k], agp_recv.at[ph, k], to_mate)
        for u in range(CHUNKS * (1 + ph)):
            sent(ps.at[u], rp_send.at[ph, u], rp_recv.at[ph, u, 0], to_mate)
            sent(qs.at[u, pl.ds(0, 3)], rr_send.at[ph, u], rr_recv.at[ph, u, 0], to_right)
    for k in range(CHUNKS):
        sent(st_x.at[pl.ds(0, 4), k], st_send.at[k], st_recv.at[k, 0], to_mate)


def per_device(dims, tokens, norm1_gain, weight_u, weight_v, scale_u, scale_v, mix_gain, spatial_weight,
               spatial_bias, weight_out, scale_out, norm2_gain, weight_up, scale_up, weight_down, scale_down):
    n_fs, n_tp = dims["fs"], dims["tp"]
    rows, width = tokens.shape
    feats = width * n_tp
    u_w, h_w = weight_u.shape[1], weight_up.shape[1]
    o_w, d_w = weight_out.shape[1], weight_down.shape[1]
    chunk = rows // CHUNKS
    block = spatial_weight.shape[1]
    n_x = n_tp // CORES
    if n_x != 4 or width != 2 * o_w or width != 2 * d_w:
        raise ValueError("unsupported mesh")
    args = (
        tokens, norm1_gain.reshape(n_fs, -1), weight_u, weight_v,
        scale_u.reshape(1, -1), scale_v.reshape(1, -1), mix_gain.reshape(1, -1), spatial_weight, spatial_bias,
        weight_out, scale_out.reshape(1, -1), norm2_gain.reshape(n_fs, -1), weight_up, scale_up.reshape(1, -1),
        weight_down, scale_down.reshape(1, -1),
    )
    def rs(units, cols):
        return [
            pltpu.VMEM((units, n_x, chunk, cols), BF),
            pltpu.VMEM((units, n_x, chunk, cols), BF),
            pltpu.VMEM((units, n_x, chunk, cols), BF),
            pltpu.VMEM((2, units, chunk // 2, cols), BF),
            pltpu.VMEM((2, units, chunk, cols), BF),
        ]

    dma = pltpu.SemaphoreType.DMA
    n_streams, units = 8, 2 * CHUNKS
    scratch = [
        pltpu.VMEM((feats, 2 * u_w), BF),
        pltpu.VMEM((n_fs, u_w, o_w), BF),
        pltpu.VMEM((feats, h_w), BF),
        pltpu.VMEM((feats, h_w), BF),
        pltpu.VMEM((n_tp, rows, width), BF),
        pltpu.VMEM((n_tp, rows, width), BF),
        pltpu.VMEM((rows, u_w), F32),
        pltpu.VMEM((u_w, rows), F32),
        pltpu.VMEM((CHUNKS, 8, chunk), F32),
        pltpu.VMEM((CHUNKS, 8, chunk), F32),
        pltpu.VMEM((CHUNKS, 8, chunk), F32),
        pltpu.VMEM((4, CHUNKS, 8, chunk), F32),
        pltpu.VMEM((rows, u_w), BF),
        pltpu.VMEM((rows, h_w), BF),
        *rs(CHUNKS, width), *rs(2 * CHUNKS, d_w),
        pltpu.VMEM((block, block), BF),
        pltpu.VMEM((block, block), F32),
        pltpu.VMEM((rows, d_w), F32),
        dma((n_streams, 2, n_fs // 2)), dma((n_streams,)), dma((n_streams,)), dma((n_streams,)),
        dma((2, CHUNKS, 6)), dma((2, CHUNKS)), dma((2, CHUNKS)), dma((2, CHUNKS)),
        dma((2, units, n_x)), dma((2, units)), dma((2, units, 6)), dma((2, units)),
        dma((CHUNKS, 4)), dma((CHUNKS,)),
    ]
    vmem = pl.BlockSpec(memory_space=pltpu.VMEM)
    return pl.pallas_call(
        functools.partial(kernel, dims),
        out_shape=jax.ShapeDtypeStruct(tokens.shape, tokens.dtype),
        in_specs=[vmem] * len(args),
        out_specs=vmem,
        scratch_shapes=scratch,
        name="layer",
        compiler_params=pltpu.CompilerParams(
            collective_id=0, has_side_effects=True, vmem_limit_bytes=64 * 1000 * 1000),
    )(*args)


def solution(mesh):
    placed = (
        P(("grp", "fs"), "tp"), P(), P("fs", "tp"), P("fs", "tp"), P("tp"), P("tp"), P("tp"), P(), P(),
        P("tp", "fs"), P("fs"), P(), P("fs", "tp"), P("tp"), P("tp", "fs"), P("fs"),
    )
    return jax.shard_map(
        functools.partial(per_device, dict(mesh.shape)), mesh=mesh, in_specs=placed,
        out_specs=P(("grp", "fs"), "tp"), check_vma=False)
```

time: 141 us -> 153 us (1.085); the launches traced: 141 us -> 151 us
  Pallas kernels: 138 us -> 149 us
    pallas_call x1, Pallas kernels: 138 us -> 149 us  [per_device(): pl.pallas_call(functools.partial(kernel, dims), out_shape=jax.ShapeDtypeS...]
where the time goes in v2:
time: 153 us; the launch traced here: 151 us
  Pallas kernels  149 us (97%)
  local copies, waits for them, and re-layouts  1.87 us (1%)
    pallas_call x1, Pallas kernels, per_device(): pl.pallas_call(functools.partial(kernel, dims), out_shape=jax.ShapeDtypeS...  149 us

profile of v2, /device:TPU:33, one launch (start us, length us, event | category | flops | bytes accessed | tf_op | source)
XLA Modules:
  0.0 150.7 jit_solution(13113560647636102858)
XLA Ops:
  0.0 148.9 %layer.1 = bf16[1024,256]{1,0:T(8,128)(2,1)} custom-call(bf16[1024,256]{1,0:T(8,128)(2,1)} %x_ref.1, f32[16,128]{1,0:T(8,128)} %bitcast.8, f32[128,128]{1,0:T(8,128)} %wu_ref.1, f32[128,128]{1,0:T(8,128)} %wv_ref.1, f32[1,128]{1,0:T(1,128)} %bitcast.11, f32[1,128]{1,0:T(1,128)} %bitcast.12, f32[1,128]{1,0:T(1,128)} %bitcast.13, f32[4,128,128]{2,1,0:T(8,128)} %sw_ref.1, ...), custom_call_target="tpu_custom_call" | custom-call | tf_op jit(solution)/shard_map/layer/pallas_call | solution.py:534
  148.9 1.9 %copy.18 = bf16[1024,256]{1,0:T(8,128)(2,1)} copy(bf16[1024,256]{1,0:T(8,128)(2,1)} %layer.1) | data formatting | bytes 1048576

commit v3 on v1

v3 whole, which is shorter than its diff:
```python
import functools

import jax
import jax.numpy as jnp
from jax import lax
from jax.experimental import pallas as pl
from jax.experimental.pallas import tpu as pltpu
from jax.sharding import PartitionSpec as P

BF = jnp.bfloat16
F32 = jnp.float32
MESH = pl.DeviceIdType.MESH
EPS = 1e-06
CORES = 2
CHUNKS = 2
ROWS = 256
SWAP = {"uv": 64, "out": 64, "up": 32, "dn": 384}
ORDER = (
    ("prep", 0), ("fe", "uvy", 1, 0), ("fe", "outy", 1, 1), ("prep", 1), ("aga", 0, 1), ("fe", "uvy", 1, 1),
    ("prep", 2), ("z", "upy", 1, 0), ("z", "upy", 1, 1), ("fo", "outy", 2, 1), ("fe", "outy", 1, 0),
    ("fe", "outy", 2, 1), ("fe", "uvy", 2, 0), ("aga", 0, 0), ("fo", "uvy", 2, 0), ("fe", "uvy", 2, 1),
    ("z", "upy", 2, 0), ("z", "upy", 2, 1), ("agb", 0, 1, 0), ("fe", "outy", 2, 0), ("fo", "uvy", 2, 1),
    ("fe", "uvy", 3, 0), ("z", "dny", 1, 0), ("fe", "outy", 3, 1), ("z", "dnb", 1, 1), ("fe", "uvy", 3, 1),
    ("fo", "uvy", 3, 1), ("agb", 0, 0, 1), ("fo", "uvy", 3, 0), ("z", "upy", 3, 1), ("z", "upy", 3, 0),
    ("z", "dny", 1, 1), ("agb", 0, 0, 0), ("fe", "uvy", 4, 0), ("fo", "outy", 2, 0), ("agb", 0, 1, 1),
    ("fo", "uvy", 4, 1), ("fo", "outy", 3, 1), ("fe", "outy", 3, 0), ("fe", "uvy", 4, 1), ("z", "dnb", 1, 0),
    ("fo", "uvy", 4, 0), ("z", "dny", 2, 0), ("z", "upb", 1, 1), ("fe", "uvy", 5, 0), ("fo", "outy", 3, 0),
    ("age", 0, 1, 0), ("agc", 0, 1, 1), ("agc", 0, 0, 1), ("fo", "uvy", 5, 0), ("fo", "uvy", 5, 1),
    ("fo", "outy", 4, 1), ("fe", "outy", 4, 0), ("agc", 0, 0, 0), ("age", 0, 0, 1), ("z", "dnb", 2, 1),
    ("agc", 0, 1, 0), ("z", "upb", 1, 0), ("fe", "uvy", 5, 1), ("age", 0, 1, 1), ("fo", "outy", 4, 0),
    ("z", "dny", 2, 1), ("fe", "outy", 4, 1), ("z", "upb", 2, 1), ("age", 0, 0, 0), ("z", "dnb", 2, 0),
    ("z", "upy", 4, 0), ("fo", "outy", 5, 0), ("z", "upy", 4, 1), ("agd", 0, 0), ("z", "dnb", 3, 1),
    ("z", "dny", 3, 0), ("yd", "uvy"), ("gating", 0), ("stats", 0), ("z", "upy", 5, 0), ("z", "upb", 2, 0),
    ("z", "upb", 3, 1), ("z", "dny", 3, 1), ("agd", 0, 1), ("gating", 1), ("fo", "outy", 5, 1), ("z", "dny", 4, 0),
    ("fe", "outy", 5, 0), ("z", "dnb", 3, 0), ("z", "upy", 5, 1), ("stats", 1), ("mixing", 0), ("aga", 2, 0),
    ("fe", "outy", 5, 1), ("z", "dnb", 4, 1), ("z", "upb", 3, 0), ("z", "upy", 6, 0), ("z", "upb", 4, 1),
    ("mixing", 1), ("aga", 2, 1), ("z", "upy", 6, 1), ("z", "dny", 5, 0), ("yd", "outy"), ("z", "dnb", 4, 0),
    ("z", "dny", 4, 1), ("z", "upy", 7, 0), ("agb", 2, 0, 1), ("agb", 2, 1, 0), ("a2s",), ("agc", 2, 0, 1),
    ("agb", 2, 1, 1), ("z", "upb", 5, 1), ("agb", 2, 0, 0), ("z", "upb", 4, 0), ("agc", 2, 1, 1), ("z", "upy", 7, 1),
    ("z", "dnb", 5, 1), ("z", "dnb", 5, 0), ("z", "upy", 8, 0), ("z", "dny", 6, 0), ("agc", 2, 0, 0),
    ("z", "dny", 5, 1), ("age", 2, 1, 0), ("z", "upb", 6, 1), ("z", "upb", 5, 0), ("age", 2, 1, 1), ("a2w",),
    ("agc", 2, 1, 0), ("z", "dnb", 6, 0), ("z", "dny", 6, 1), ("z", "dny", 7, 0), ("z", "dnb", 6, 1), ("agd", 2, 1),
    ("z", "upy", 9, 0), ("outp", 1), ("age", 2, 0, 1), ("aga", 1, 1), ("z", "upb", 7, 1), ("z", "upb", 6, 0),
    ("z", "dny", 7, 1), ("age", 2, 0, 0), ("z", "upy", 8, 1), ("z", "dny", 8, 0), ("z", "dnb", 7, 1), ("agd", 2, 0),
    ("agb", 1, 1, 1), ("agb", 1, 1, 0), ("z", "upb", 7, 0), ("outp", 0), ("z", "upb", 8, 1), ("agc", 1, 1, 1),
    ("agc", 1, 1, 0), ("aga", 1, 0), ("z", "dny", 9, 0), ("age", 1, 1, 0), ("z", "dny", 8, 1), ("z", "dnb", 7, 0),
    ("z", "dnb", 8, 1), ("age", 1, 1, 1), ("agd", 1, 1), ("yd", "upy"), ("z", "upb", 9, 1), ("agb", 1, 0, 1),
    ("agb", 1, 0, 0), ("z", "upb", 8, 0), ("ffup", 1), ("z", "dnb", 8, 0), ("z", "dnb", 9, 1), ("yd", "dny"),
    ("rsa", 1, 0), ("rsa", 1, 1), ("rsb", 1, 0), ("age", 1, 0, 1), ("agc", 1, 0, 1), ("agc", 1, 0, 0),
    ("age", 1, 0, 0), ("rsb", 1, 1), ("agd", 1, 0), ("ffup", 0), ("rsc", 1, 0), ("rsc", 1, 1), ("rsa", 0, 0),
    ("rsa", 0, 1), ("rsb", 0, 0), ("rsb", 0, 1), ("rsd", 1), ("rsc", 0, 1), ("rsc", 0, 0), ("rsd", 0),
)


class Stream:
    def __init__(self, name, ref, rows, whole, paired):
        self.name, self.ref, self.rows, self.whole, self.paired = name, ref, rows, whole, paired


def kernel(
    dims,
    x_ref, g1_ref, wu_ref, wv_ref, su_ref, sv_ref, mg_ref, sw_ref, sb_ref, wo_ref, so_ref,
    g2_ref, wup_ref, sup_ref, wdn_ref, sdn_ref,
    out_ref,
    wuv, wout, wup, wdn, xg, rg, gg, wmix, ub, vt, st_own, st_p, st_c, st_x, hid,
    ps, pr, qs, op, fi, mask, bias,
    z_recv, z_send, y_recv, y_send, ag_recv, ag_send, agp_recv, agp_send,
    rp_recv, rp_send, rr_recv, rr_send, st_recv, st_send, a2_recv, a2_send,
):
    n_fs, n_tp = dims["fs"], dims["tp"]
    n_x = n_tp // CORES
    half_ring = n_fs // 2
    total_rows, width = x_ref.shape
    feats = width * n_tp
    u_w = wu_ref.shape[1]
    k_fs = wu_ref.shape[0]
    h_w = wup_ref.shape[1]
    gm_w = u_w * n_tp
    chunk = total_rows // CHUNKS
    half = chunk // 2
    block = sw_ref.shape[1]
    pair = dims["grp"] % 2 == 0

    g = lax.axis_index("grp")
    f = lax.axis_index("fs")
    t = lax.axis_index("tp")
    cx = t // CORES
    core = t % CORES
    par = g % 2

    def chip(d):
        return (cx + d) % n_x

    def tp_of(d):
        return chip(d) * CORES + core

    to_right, to_left, to_opp = {"tp": tp_of(1)}, {"tp": tp_of(n_x - 1)}, {"tp": tp_of(2)}
    to_mate = {"tp": cx * CORES + 1 - core}
    to_up, to_down = {"fs": (f + 1) % n_fs}, {"fs": (f + n_fs - 1) % n_fs}
    to_pair = {"grp": g + 1 - 2 * par}

    to_up2, to_down2 = {"fs": (f + 2) % n_fs}, {"fs": (f + n_fs - 2) % n_fs}
    others = [{"tp": chip(rel) * CORES + (core + c) % CORES} for rel in range(n_x) for c in range(CORES) if rel or c]
    neighbours = others + [to_up, to_down, to_up2, to_down2]
    if pair:
        neighbours.append(to_pair)
    barrier = pltpu.get_barrier_semaphore()
    for n in neighbours:
        pl.semaphore_signal(barrier, inc=1, device_id=n, device_id_type=MESH)
    pl.semaphore_wait(barrier, len(neighbours))

    def rcopy(src, dst, ss, rs, dev):
        return pltpu.make_async_remote_copy(
            src_ref=src, dst_ref=dst, send_sem=ss, recv_sem=rs, device_id=dev, device_id_type=MESH)

    def got(ref, sem, spare, dev):
        rcopy(ref, ref, spare, sem, dev).wait_recv()

    def sent(ref, sem, spare, dev):
        rcopy(ref, ref, sem, spare, dev).wait_send()

    def rows_2d(ref, start):
        def at(slot, rows):
            return ref.at[pl.ds(pl.multiple_of(slot * k_fs + start, 16), rows), :]
        return at

    def rows_3d(ref, start):
        def at(slot, rows):
            return ref.at[slot, pl.ds(pl.multiple_of(start, 16), rows), :]
        return at

    def whole_2d(ref, rows):
        return ref.at[pl.ds(0, (n_fs - 1) * rows), :]

    def whole_3d(ref, rows):
        return ref.at[pl.ds(0, n_fs - 1), pl.ds(0, rows), :]

    def make(name, ref, three, first, own_rows, swap):
        def at(r, start):
            return (rows_3d if three else rows_2d)(r, first + start)

        whole = whole_3d if three else whole_2d
        result = []
        if pair and swap:
            shared = own_rows - 2 * swap
            result.append(Stream(name + "y", at(ref, par * (own_rows - swap)), swap, whole(ref, swap), True))
            if shared:
                result.append(Stream(name + "b", at(ref, swap), shared, whole(ref, shared), False))
        else:
            result.append(Stream(name + "y", at(ref, 0), own_rows, whole(ref, own_rows), False))
        return result

    streams = {}
    for s in (make("uv", wuv, False, 0, k_fs, SWAP["uv"]) + make("out", wout, True, 0, u_w, SWAP["out"])
              + make("up", wup, False, 0, k_fs, SWAP["up"]) + make("dn", wdn, True, 0, h_w, SWAP["dn"])):
        s.index = len(streams)
        streams[s.name] = s

    def z_dirs(s, hop):
        return (0, 1) if hop < half_ring else (s.index % 2,)

    def piece_at(s, d, back):
        return s.ref((f + (n_fs - back if d == 0 else back)) % n_fs, s.rows)

    def z_got(s, d, hop):
        piece = piece_at(s, d, hop)
        got(piece, z_recv.at[s.index, d, hop - 1], z_send.at[s.index], to_up)
        return piece

    def z_send_on(s, d, back, hop, to):
        piece = piece_at(s, d, back)
        rcopy(piece, piece, z_send.at[s.index], z_recv.at[s.index, d, hop - 1], to).start()

    def to_partner(s, piece):
        if s.paired:
            rcopy(piece, piece, y_send.at[s.index], y_recv.at[s.index], to_pair).start()

    def z_hop(name, hop, d):
        s = streams[name]
        if hop > 1 and d in z_dirs(s, hop - 1):
            to_partner(s, z_got(s, d, hop - 1))
        if hop <= half_ring and d in z_dirs(s, hop):
            z_send_on(s, d, hop - 1, hop, to_down if d else to_up)

    def z_even(name, stage, d):
        s = streams[name]
        even = 2 * (stage - 1)
        arrived = stage > 1 and d in z_dirs(s, even)
        if arrived:
            piece = z_got(s, d, even)
        if even < half_ring:
            for step, to in ((2, to_down2 if d else to_up2), (1, to_down if d else to_up)):
                if d in z_dirs(s, even + step):
                    z_send_on(s, d, even, even + step, to)
        if arrived:
            to_partner(s, piece)

    def z_odd(name, stage, d):
        s = streams[name]
        to_partner(s, z_got(s, d, 2 * stage - 3))

    def y_done(name):
        s = streams[name]
        if not s.paired:
            return
        got(s.whole, y_recv.at[s.index], y_send.at[s.index], to_pair)

    def ag_rows(buf, slot, start, rows):
        return buf.at[slot, pl.ds(start, rows), :]

    gathered = (xg, rg, gg)

    def to_other_core(ph, k, piece):
        rcopy(piece, piece, agp_send.at[ph, k], agp_recv.at[ph, k], to_mate).start()

    def ag_a(ph, k):
        buf = gathered[ph]

        def src(at, n):
            return x_ref.at[pl.ds(at, n), :] if ph == 0 else ag_rows(buf, t, at, n)

        for n, to, lo in ((0, to_right, 0), (1, to_right, half), (2, to_left, half), (3, to_left, 0)):
            at = k * chunk + lo
            rcopy(src(at, half), ag_rows(buf, t, at, half), ag_send.at[ph, k], ag_recv.at[ph, k, n], to).start()
        at = k * chunk
        rcopy(src(at, chunk), ag_rows(buf, t, at, chunk), agp_send.at[ph, k], agp_recv.at[ph, k], to_mate).start()

    SIDES = ((n_x - 1, 0, to_right), (1, half, to_left))

    def ag_b(ph, k, side):
        chip_at, lo, to = SIDES[side]
        part = ag_rows(gathered[ph], tp_of(chip_at), k * chunk + lo, half)
        got(part, ag_recv.at[ph, k, 2 * side], ag_send.at[ph, k], to)
        rcopy(part, part, ag_send.at[ph, k], ag_recv.at[ph, k, 4 + side], to).start()

    def ag_c(ph, k, side):
        chip_at, lo, to = SIDES[side]
        part = ag_rows(gathered[ph], tp_of(chip_at), k * chunk + half - lo, half)
        got(part, ag_recv.at[ph, k, 2 * side + 1], ag_send.at[ph, k], to)
        to_other_core(ph, k, ag_rows(gathered[ph], tp_of(chip_at), k * chunk, chunk))

    def ag_e(ph, k, side):
        part = ag_rows(gathered[ph], tp_of(2), k * chunk + SIDES[side][1], half)
        got(part, ag_recv.at[ph, k, 4 + side], ag_send.at[ph, k], to_right)
        to_other_core(ph, k, part)

    def ag_d(ph, k):
        got(gathered[ph].at[pl.ds(0, n_x), pl.ds(k * chunk, chunk), :], agp_recv.at[ph, k], agp_send.at[ph, k], to_mate)

    def a2_s():
        for n, to in enumerate(others):
            rcopy(wout.at[pl.ds(2 * to["tp"], 2)], wmix.at[t], a2_send.at[0], a2_recv.at[0], to).start()
        wmix[t] = wout[pl.ds(2 * t, 2)]

    def a2_w():
        got(wmix.at[pl.ds(0, n_tp - 1)], a2_recv.at[0], a2_send.at[0], to_mate)

    def out_p(k):
        rows = pl.ds(k * chunk, chunk)
        left = jnp.concatenate([gg[j, rows, :] for j in range(n_tp)], axis=1)
        right = jnp.concatenate(
            [jnp.concatenate([wmix[j, 0], wmix[j, 1]], axis=1) for j in range(n_tp)], axis=0)
        total = jnp.dot(left, right, preferred_element_type=F32)
        rg[t, rows, :] = (x_ref[rows, :].astype(F32) + total).astype(BF)

    PAIRS = ((2, 1), (3, 0))

    def product(k, rel, c):
        j = chip(rel) * CORES + c
        right = jnp.concatenate([wdn[2 * j], wdn[2 * j + 1]], axis=1)
        return jnp.dot(hid[pl.ds(k * chunk, chunk), :], right, preferred_element_type=F32)

    def rs_a(k, p):
        for rel in PAIRS[p]:
            ps[k, rel] = product(k, rel, 1 - core).astype(BF)
            rcopy(ps.at[k, rel], pr.at[k, rel], rp_send.at[k], rp_recv.at[k, rel], to_mate).start()

    def rs_b(k, p):
        ss = rr_send.at[k]
        for rel in PAIRS[p]:
            got(pr.at[k, rel], rp_recv.at[k, rel], rp_send.at[k], to_mate)
            qs[k, rel] = (product(k, rel, core) + pr[k, rel].astype(F32)).astype(BF)
            low, high = qs.at[k, rel, pl.ds(0, half), :], qs.at[k, rel, pl.ds(half, half), :]
            if rel == 2:
                rcopy(low, op.at[0, k], ss, rr_recv.at[k, 0], to_right).start()
                rcopy(high, op.at[1, k], ss, rr_recv.at[k, 1], to_left).start()
            elif rel == 1:
                rcopy(high, fi.at[0, k, pl.ds(half, half), :], ss, rr_recv.at[k, 2], to_right).start()
            elif rel == 3:
                rcopy(low, fi.at[1, k, pl.ds(0, half), :], ss, rr_recv.at[k, 3], to_left).start()

    def rs_c(k, side):
        ss = rr_send.at[k]
        rel, (_, lo, to) = (1, 3)[side], SIDES[side]
        got(op.at[side, k], rr_recv.at[k, side], ss, to)
        rows = pl.ds(lo, half)
        qs[k, rel, rows, :] = (qs[k, rel, rows, :].astype(F32) + op[side, k].astype(F32)).astype(BF)
        rcopy(qs.at[k, rel, rows, :], fi.at[side, k, rows, :], ss, rr_recv.at[k, 4 + side], to).start()

    def rs_d(k):
        ss = rr_send.at[k]
        for n, side, lo in ((2, 0, half), (3, 1, 0), (4, 0, 0), (5, 1, half)):
            got(fi.at[side, k, pl.ds(lo, half), :], rr_recv.at[k, n], ss, to_right)
        for r in range(0, chunk, ROWS):
            rows, at = pl.ds(r, ROWS), pl.ds(k * chunk + r, ROWS)
            total = qs[k, 0, rows, :].astype(F32) + fi[0, k, rows, :].astype(F32) + fi[1, k, rows, :].astype(F32)
            out_ref[at, :] = (rg[t, at, :].astype(F32) + total).astype(BF)

    def column(row):
        return jnp.broadcast_to(row, (row.shape[1], row.shape[1])).T

    def joined(buf, r):
        parts = [buf[j, pl.ds(r, ROWS), :] for j in range(n_tp)]
        squares = None
        for part in parts:
            wide = part.astype(F32)
            squares = wide * wide if squares is None else squares + wide * wide
        inv = lax.rsqrt(jnp.sum(squares, axis=1, keepdims=True) / feats + EPS)
        return jnp.concatenate(parts, axis=1), inv

    def gating(k):
        scale_uv = jnp.concatenate([su_ref[...], sv_ref[...]], axis=1)
        for r in range(0, chunk, ROWS):
            at = k * chunk + r
            lhs, inv = joined(xg, at)
            pre = jnp.dot(lhs, wuv[...], preferred_element_type=F32) * inv * scale_uv
            act = jax.nn.gelu(pre)
            ub[pl.ds(at, ROWS), :] = act[:, :u_w]
            turned = act[:, u_w:].T
            vt[:, pl.ds(at, ROWS)] = turned
            st_own[k, :, pl.ds(r, ROWS)] = jnp.concatenate(
                [jnp.sum(turned, axis=0, keepdims=True), jnp.sum(turned * turned, axis=0, keepdims=True),
                 jnp.zeros((6, ROWS), F32)], axis=0)
        rcopy(st_own.at[k], st_p.at[k], st_send.at[k], st_recv.at[k, 3], to_mate).start()

    def stats(k):
        got(st_p.at[k], st_recv.at[k, 3], st_send.at[k], to_mate)
        st_c[k] = st_own[k] + st_p[k]
        for n, to in enumerate((to_right, to_left, to_opp)):
            rcopy(st_c.at[k], st_x.at[n, k], st_send.at[k], st_recv.at[k, n], to).start()

    def mixing(k):
        for n in range(3):
            got(st_x.at[n, k], st_recv.at[k, n], st_send.at[k], to_mate)
        total = st_c[k] + st_x[0, k] + st_x[1, k] + st_x[2, k]
        mean = total[0:1] / gm_w
        square = total[1:2] / gm_w
        scale = lax.rsqrt(square - mean * mean + EPS)
        gain = column(mg_ref[...])[:, 0:1]
        for b in range(0, chunk, block):
            at = k * chunk + b
            v_norm = ((vt[:, pl.ds(at, block)] - mean[:, b:b + block]) * scale[:, b:b + block] * gain).astype(BF)
            mixed = lax.dot_general(mask[...], v_norm, (((1,), (1,)), ((), ())), preferred_element_type=F32)
            gg[t, pl.ds(at, block), :] = (ub[pl.ds(at, block), :] * (mixed + bias[...])).astype(BF)

    def ff_up(k):
        for r in range(0, chunk, ROWS):
            at = k * chunk + r
            lhs, inv = joined(rg, at)
            for n in range(0, h_w, 256):
                cols = pl.ds(n, 256)
                acc = jnp.dot(lhs, wup[:, n:n + 256], preferred_element_type=F32)
                acc = jnp.maximum(acc * inv * sup_ref[:, n:n + 256], 0.0)
                hid[pl.ds(at, ROWS), cols] = (acc * acc).astype(BF)

    def rounded(w):
        return w.astype(BF).astype(F32)

    own = pl.ds(pl.multiple_of(f * k_fs, k_fs), k_fs)

    def prep(n):
        if n == 0:
            g1 = column(g1_ref[pl.ds(f, 1), :])
            wuv[own, :] = (jnp.concatenate([rounded(wu_ref[...]) * g1, rounded(wv_ref[...]) * g1], axis=1)).astype(BF)
            wout[f] = (rounded(wo_ref[...]) * so_ref[...]).astype(BF)
        elif n == 1:
            g2 = column(g2_ref[pl.ds(f, 1), :])[:, 0:1]
            wup[own, :] = (rounded(wup_ref[...]) * g2).astype(BF)
        else:
            wdn[f] = (rounded(wdn_ref[...]) * sdn_ref[...]).astype(BF)
            xg[t] = x_ref[...]
            at = lax.broadcasted_iota(jnp.int32, (block, block), 0)
            low = at >= lax.broadcasted_iota(jnp.int32, (block, block), 1)
            grp_at = t * u_w // (gm_w // sw_ref.shape[0])
            mask[...] = jnp.where(low, sw_ref[grp_at], 0.0).astype(BF)
            bias[...] = column(sb_ref[pl.ds(grp_at, 1), :])

    steps = {
        "prep": prep, "z": z_hop, "fe": z_even, "fo": z_odd, "yd": y_done, "aga": ag_a, "agb": ag_b, "agc": ag_c,
        "age": ag_e, "agd": ag_d, "gating": gating, "stats": stats, "mixing": mixing, "a2s": a2_s, "a2w": a2_w,
        "outp": out_p, "ffup": ff_up, "rsa": rs_a, "rsb": rs_b, "rsc": rs_c, "rsd": rs_d,
    }
    for name, *rest in ORDER:
        steps[name](*rest)

    for s in streams.values():
        sent(s.whole, z_send.at[s.index], z_recv.at[s.index, 0, 0], to_up)
        if s.paired:
            sent(s.whole, y_send.at[s.index], y_recv.at[s.index], to_pair)
    for ph, buf in enumerate(gathered):
        for k in range(CHUNKS):
            rows = pl.ds(k * chunk, chunk)
            sent(buf.at[pl.ds(0, 3), rows, :], ag_send.at[ph, k], ag_recv.at[ph, k, 0], to_right)
            sent(buf.at[pl.ds(0, n_x), rows, :], agp_send.at[ph, k], agp_recv.at[ph, k], to_mate)
    for k in range(CHUNKS):
        sent(ps.at[k], rp_send.at[k], rp_recv.at[k, 0], to_mate)
        sent(qs.at[k, pl.ds(0, 3)], rr_send.at[k], rr_recv.at[k, 0], to_right)
        sent(st_x.at[pl.ds(0, 4), k], st_send.at[k], st_recv.at[k, 0], to_mate)
    sent(wmix.at[pl.ds(0, n_tp - 1)], a2_send.at[0], a2_recv.at[0], to_mate)


def per_device(dims, tokens, norm1_gain, weight_u, weight_v, scale_u, scale_v, mix_gain, spatial_weight,
               spatial_bias, weight_out, scale_out, norm2_gain, weight_up, scale_up, weight_down, scale_down):
    n_fs, n_tp = dims["fs"], dims["tp"]
    rows, width = tokens.shape
    feats = width * n_tp
    u_w, h_w = weight_u.shape[1], weight_up.shape[1]
    o_w, d_w = weight_out.shape[1], weight_down.shape[1]
    chunk = rows // CHUNKS
    block = spatial_weight.shape[1]
    n_x = n_tp // CORES
    if n_x != 4 or width != 2 * o_w or width != 2 * d_w:
        raise ValueError("unsupported mesh")
    args = (
        tokens, norm1_gain.reshape(n_fs, -1), weight_u, weight_v,
        scale_u.reshape(1, -1), scale_v.reshape(1, -1), mix_gain.reshape(1, -1), spatial_weight, spatial_bias,
        weight_out, scale_out.reshape(1, -1), norm2_gain.reshape(n_fs, -1), weight_up, scale_up.reshape(1, -1),
        weight_down, scale_down.reshape(1, -1),
    )
    dma = pltpu.SemaphoreType.DMA
    n_streams = 8
    scratch = [
        pltpu.VMEM((feats, 2 * u_w), BF),
        pltpu.VMEM((n_fs, u_w, o_w), BF),
        pltpu.VMEM((feats, h_w), BF),
        pltpu.VMEM((n_fs, h_w, d_w), BF),
        pltpu.VMEM((n_tp, rows, width), BF),
        pltpu.VMEM((n_tp, rows, width), BF),
        pltpu.VMEM((n_tp, rows, u_w), BF),
        pltpu.VMEM((n_tp, 2, u_w, o_w), BF),
        pltpu.VMEM((rows, u_w), F32),
        pltpu.VMEM((u_w, rows), F32),
        pltpu.VMEM((CHUNKS, 8, chunk), F32),
        pltpu.VMEM((CHUNKS, 8, chunk), F32),
        pltpu.VMEM((CHUNKS, 8, chunk), F32),
        pltpu.VMEM((4, CHUNKS, 8, chunk), F32),
        pltpu.VMEM((rows, h_w), BF),
        pltpu.VMEM((CHUNKS, n_x, chunk, width), BF),
        pltpu.VMEM((CHUNKS, n_x, chunk, width), BF),
        pltpu.VMEM((CHUNKS, n_x, chunk, width), BF),
        pltpu.VMEM((2, CHUNKS, chunk // 2, width), BF),
        pltpu.VMEM((2, CHUNKS, chunk, width), BF),
        pltpu.VMEM((block, block), BF),
        pltpu.VMEM((block, block), F32),
        dma((n_streams, 2, n_fs // 2)), dma((n_streams,)), dma((n_streams,)), dma((n_streams,)),
        dma((3, CHUNKS, 6)), dma((3, CHUNKS)), dma((3, CHUNKS)), dma((3, CHUNKS)),
        dma((CHUNKS, n_x)), dma((CHUNKS,)), dma((CHUNKS, 6)), dma((CHUNKS,)),
        dma((CHUNKS, 4)), dma((CHUNKS,)), dma((1,)), dma((1,)),
    ]
    vmem = pl.BlockSpec(memory_space=pltpu.VMEM)
    return pl.pallas_call(
        functools.partial(kernel, dims),
        out_shape=jax.ShapeDtypeStruct(tokens.shape, tokens.dtype),
        in_specs=[vmem] * len(args),
        out_specs=vmem,
        scratch_shapes=scratch,
        name="layer",
        compiler_params=pltpu.CompilerParams(
            collective_id=0, has_side_effects=True, vmem_limit_bytes=64 * 1000 * 1000),
    )(*args)


def solution(mesh):
    placed = (
        P(("grp", "fs"), "tp"), P(), P("fs", "tp"), P("fs", "tp"), P("tp"), P("tp"), P("tp"), P(), P(),
        P("tp", "fs"), P("fs"), P(), P("fs", "tp"), P("tp"), P("tp", "fs"), P("fs"),
    )
    return jax.shard_map(
        functools.partial(per_device, dict(mesh.shape)), mesh=mesh, in_specs=placed,
        out_specs=P(("grp", "fs"), "tp"), check_vma=False)
```

time: 141 us -> 130 us (0.922)
  Pallas kernels: 138 us -> 128 us
    pallas_call x1, Pallas kernels: 138 us -> 128 us  [per_device(): pl.pallas_call(functools.partial(kernel, dims), out_shape=jax.ShapeDtypeS...]
where the time goes in v3:
time: 130 us
  Pallas kernels  128 us (98%)
  local copies, waits for them, and re-layouts  1.87 us (1%)
    pallas_call x1, Pallas kernels, per_device(): pl.pallas_call(functools.partial(kernel, dims), out_shape=jax.ShapeDtypeS...  128 us

profile of v3, /device:TPU:33, one launch (start us, length us, event | category | flops | bytes accessed | tf_op | source)
XLA Modules:
  0.0 129.9 jit_solution(12282222947200964723)
XLA Ops:
  0.0 128.0 %layer.1 = bf16[1024,256]{1,0:T(8,128)(2,1)} custom-call(bf16[1024,256]{1,0:T(8,128)(2,1)} %x_ref.1, f32[16,128]{1,0:T(8,128)} %bitcast.8, f32[128,128]{1,0:T(8,128)} %wu_ref.1, f32[128,128]{1,0:T(8,128)} %wv_ref.1, f32[1,128]{1,0:T(1,128)} %bitcast.11, f32[1,128]{1,0:T(1,128)} %bitcast.12, f32[1,128]{1,0:T(1,128)} %bitcast.13, f32[4,128,128]{2,1,0:T(8,128)} %sw_ref.1, ...), custom_call_target="tpu_custom_call" | custom-call | tf_op jit(solution)/shard_map/layer/pallas_call | solution.py:461
  128.0 1.9 %copy.18 = bf16[1024,256]{1,0:T(8,128)(2,1)} copy(bf16[1024,256]{1,0:T(8,128)(2,1)} %layer.1) | data formatting | bytes 1048576

commit v4 on v3

--- a/solution.py
+++ b/solution.py
@@ -14,41 +14,48 @@
 CORES = 2
 CHUNKS = 2
 ROWS = 256
-SWAP = {"uv": 64, "out": 64, "up": 32, "dn": 384}
+SWAP = {"uv": 64, "out": 64, "up": 48, "e": 16, "f": 16}
 ORDER = (
-    ("prep", 0), ("fe", "uvy", 1, 0), ("fe", "outy", 1, 1), ("prep", 1), ("aga", 0, 1), ("fe", "uvy", 1, 1),
-    ("prep", 2), ("z", "upy", 1, 0), ("z", "upy", 1, 1), ("fo", "outy", 2, 1), ("fe", "outy", 1, 0),
-    ("fe", "outy", 2, 1), ("fe", "uvy", 2, 0), ("aga", 0, 0), ("fo", "uvy", 2, 0), ("fe", "uvy", 2, 1),
-    ("z", "upy", 2, 0), ("z", "upy", 2, 1), ("agb", 0, 1, 0), ("fe", "outy", 2, 0), ("fo", "uvy", 2, 1),
-    ("fe", "uvy", 3, 0), ("z", "dny", 1, 0), ("fe", "outy", 3, 1), ("z", "dnb", 1, 1), ("fe", "uvy", 3, 1),
-    ("fo", "uvy", 3, 1), ("agb", 0, 0, 1), ("fo", "uvy", 3, 0), ("z", "upy", 3, 1), ("z", "upy", 3, 0),
-    ("z", "dny", 1, 1), ("agb", 0, 0, 0), ("fe", "uvy", 4, 0), ("fo", "outy", 2, 0), ("agb", 0, 1, 1),
-    ("fo", "uvy", 4, 1), ("fo", "outy", 3, 1), ("fe", "outy", 3, 0), ("fe", "uvy", 4, 1), ("z", "dnb", 1, 0),
-    ("fo", "uvy", 4, 0), ("z", "dny", 2, 0), ("z", "upb", 1, 1), ("fe", "uvy", 5, 0), ("fo", "outy", 3, 0),
-    ("age", 0, 1, 0), ("agc", 0, 1, 1), ("agc", 0, 0, 1), ("fo", "uvy", 5, 0), ("fo", "uvy", 5, 1),
-    ("fo", "outy", 4, 1), ("fe", "outy", 4, 0), ("agc", 0, 0, 0), ("age", 0, 0, 1), ("z", "dnb", 2, 1),
-    ("agc", 0, 1, 0), ("z", "upb", 1, 0), ("fe", "uvy", 5, 1), ("age", 0, 1, 1), ("fo", "outy", 4, 0),
-    ("z", "dny", 2, 1), ("fe", "outy", 4, 1), ("z", "upb", 2, 1), ("age", 0, 0, 0), ("z", "dnb", 2, 0),
-    ("z", "upy", 4, 0), ("fo", "outy", 5, 0), ("z", "upy", 4, 1), ("agd", 0, 0), ("z", "dnb", 3, 1),
-    ("z", "dny", 3, 0), ("yd", "uvy"), ("gating", 0), ("stats", 0), ("z", "upy", 5, 0), ("z", "upb", 2, 0),
-    ("z", "upb", 3, 1), ("z", "dny", 3, 1), ("agd", 0, 1), ("gating", 1), ("fo", "outy", 5, 1), ("z", "dny", 4, 0),
-    ("fe", "outy", 5, 0), ("z", "dnb", 3, 0), ("z", "upy", 5, 1), ("stats", 1), ("mixing", 0), ("aga", 2, 0),
-    ("fe", "outy", 5, 1), ("z", "dnb", 4, 1), ("z", "upb", 3, 0), ("z", "upy", 6, 0), ("z", "upb", 4, 1),
-    ("mixing", 1), ("aga", 2, 1), ("z", "upy", 6, 1), ("z", "dny", 5, 0), ("yd", "outy"), ("z", "dnb", 4, 0),
-    ("z", "dny", 4, 1), ("z", "upy", 7, 0), ("agb", 2, 0, 1), ("agb", 2, 1, 0), ("a2s",), ("agc", 2, 0, 1),
-    ("agb", 2, 1, 1), ("z", "upb", 5, 1), ("agb", 2, 0, 0), ("z", "upb", 4, 0), ("agc", 2, 1, 1), ("z", "upy", 7, 1),
-    ("z", "dnb", 5, 1), ("z", "dnb", 5, 0), ("z", "upy", 8, 0), ("z", "dny", 6, 0), ("agc", 2, 0, 0),
-    ("z", "dny", 5, 1), ("age", 2, 1, 0), ("z", "upb", 6, 1), ("z", "upb", 5, 0), ("age", 2, 1, 1), ("a2w",),
-    ("agc", 2, 1, 0), ("z", "dnb", 6, 0), ("z", "dny", 6, 1), ("z", "dny", 7, 0), ("z", "dnb", 6, 1), ("agd", 2, 1),
-    ("z", "upy", 9, 0), ("outp", 1), ("age", 2, 0, 1), ("aga", 1, 1), ("z", "upb", 7, 1), ("z", "upb", 6, 0),
-    ("z", "dny", 7, 1), ("age", 2, 0, 0), ("z", "upy", 8, 1), ("z", "dny", 8, 0), ("z", "dnb", 7, 1), ("agd", 2, 0),
-    ("agb", 1, 1, 1), ("agb", 1, 1, 0), ("z", "upb", 7, 0), ("outp", 0), ("z", "upb", 8, 1), ("agc", 1, 1, 1),
-    ("agc", 1, 1, 0), ("aga", 1, 0), ("z", "dny", 9, 0), ("age", 1, 1, 0), ("z", "dny", 8, 1), ("z", "dnb", 7, 0),
-    ("z", "dnb", 8, 1), ("age", 1, 1, 1), ("agd", 1, 1), ("yd", "upy"), ("z", "upb", 9, 1), ("agb", 1, 0, 1),
-    ("agb", 1, 0, 0), ("z", "upb", 8, 0), ("ffup", 1), ("z", "dnb", 8, 0), ("z", "dnb", 9, 1), ("yd", "dny"),
-    ("rsa", 1, 0), ("rsa", 1, 1), ("rsb", 1, 0), ("age", 1, 0, 1), ("agc", 1, 0, 1), ("agc", 1, 0, 0),
-    ("age", 1, 0, 0), ("rsb", 1, 1), ("agd", 1, 0), ("ffup", 0), ("rsc", 1, 0), ("rsc", 1, 1), ("rsa", 0, 0),
-    ("rsa", 0, 1), ("rsb", 0, 0), ("rsb", 0, 1), ("rsd", 1), ("rsc", 0, 1), ("rsc", 0, 0), ("rsd", 0),
+    ("prep", 0), ("z", "outy", 1, 0), ("aga", 0, 1), ("z", "outy", 1, 1), ("fe", "uvy", 1, 0), ("prep", 1),
+    ("z", "upy", 1, 0), ("fe", "uvy", 1, 1), ("prep", 2), ("z", "outy", 2, 1), ("z", "outy", 2, 0), ("aga", 0, 0),
+    ("z", "upb", 1, 1), ("z", "ey", 1, 1), ("fo", "uvy", 2, 0), ("fe", "uvy", 2, 0), ("agb", 0, 1, 0),
+    ("z", "outy", 3, 1), ("agb", 0, 1, 1), ("fo", "uvy", 2, 1), ("fe", "uvy", 2, 1), ("z", "upy", 2, 0),
+    ("z", "upy", 1, 1), ("z", "outy", 4, 1), ("z", "outy", 3, 0), ("fe", "uvy", 3, 0), ("fe", "uvy", 3, 1),
+    ("agb", 0, 0, 1), ("fo", "uvy", 3, 1), ("fo", "uvy", 3, 0), ("z", "upb", 1, 0), ("z", "outy", 4, 0),
+    ("z", "ey", 1, 0), ("z", "outy", 5, 1), ("agc", 0, 1, 0), ("z", "eb", 1, 1), ("fo", "uvy", 4, 0),
+    ("agb", 0, 0, 0), ("fe", "uvy", 4, 0), ("z", "ey", 2, 1), ("agc", 0, 0, 1), ("fo", "uvy", 4, 1),
+    ("fe", "uvy", 4, 1), ("z", "outy", 5, 0), ("z", "outy", 6, 1), ("z", "upb", 2, 1), ("z", "upb", 2, 0),
+    ("z", "eb", 1, 0), ("z", "fb", 1, 1), ("fo", "uvy", 5, 1), ("age", 0, 1, 1), ("fe", "uvy", 5, 0),
+    ("agc", 0, 1, 1), ("fo", "uvy", 5, 0), ("age", 0, 1, 0), ("z", "outy", 7, 1), ("z", "outy", 6, 0),
+    ("age", 0, 0, 0), ("z", "upy", 3, 0), ("z", "ey", 3, 1), ("z", "upy", 2, 1), ("agc", 0, 0, 0),
+    ("z", "outy", 8, 1), ("z", "eb", 2, 1), ("agd", 0, 1), ("age", 0, 0, 1), ("z", "ey", 2, 0), ("z", "outy", 7, 0),
+    ("z", "fb", 1, 0), ("z", "upb", 3, 1), ("z", "upb", 3, 0), ("yd", "uvy"), ("gating", 1), ("agd", 0, 0),
+    ("gating", 0), ("z", "outy", 9, 1), ("z", "outy", 8, 0), ("z", "upy", 3, 1), ("z", "fb", 2, 1), ("z", "ey", 3, 0),
+    ("z", "upy", 4, 0), ("z", "eb", 2, 0), ("mixing", 1), ("aga", 2, 1), ("z", "fy", 1, 0), ("z", "ey", 4, 0),
+    ("z", "eb", 3, 1), ("mixing", 0), ("z", "upy", 4, 1), ("yd", "outy"), ("z", "ey", 4, 1), ("aga", 2, 0),
+    ("z", "upy", 5, 0), ("agb", 2, 1, 0), ("z", "fy", 1, 1), ("a2s",), ("z", "eb", 4, 1), ("agb", 2, 1, 1),
+    ("z", "upb", 4, 0), ("z", "eb", 3, 0), ("z", "ey", 5, 0), ("z", "upy", 5, 1), ("z", "upy", 6, 0),
+    ("z", "fb", 3, 1), ("z", "ey", 5, 1), ("agc", 2, 1, 1), ("z", "upb", 4, 1), ("z", "eb", 4, 0), ("z", "ey", 6, 0),
+    ("agc", 2, 1, 0), ("z", "fb", 2, 0), ("z", "upy", 6, 1), ("age", 2, 1, 0), ("agb", 2, 0, 1), ("agc", 2, 0, 1),
+    ("z", "ey", 6, 1), ("age", 2, 1, 1), ("z", "upy", 7, 0), ("agb", 2, 0, 0), ("agd", 2, 1), ("z", "ey", 7, 0),
+    ("z", "upb", 5, 1), ("age", 2, 0, 1), ("z", "fy", 2, 0), ("z", "upb", 5, 0), ("z", "upy", 7, 1),
+    ("z", "ey", 7, 1), ("a2w",), ("outp", 1), ("agc", 2, 0, 0), ("z", "eb", 5, 1), ("aga", 1, 1), ("z", "upy", 8, 0),
+    ("age", 2, 0, 0), ("z", "upb", 6, 1), ("z", "ey", 8, 0), ("fe", "uvy", 5, 1), ("z", "fy", 3, 0), ("agd", 2, 0),
+    ("outp", 0), ("z", "fb", 4, 1), ("z", "fb", 3, 0), ("z", "upy", 8, 1), ("z", "eb", 5, 0), ("agb", 1, 1, 0),
+    ("z", "upy", 9, 0), ("agb", 1, 1, 1), ("z", "ey", 8, 1), ("aga", 1, 0), ("z", "fy", 2, 1), ("z", "eb", 6, 1),
+    ("z", "ey", 9, 0), ("z", "fy", 4, 0), ("z", "upb", 6, 0), ("z", "upb", 7, 1), ("z", "fb", 4, 0), ("agc", 1, 1, 0),
+    ("z", "fy", 3, 1), ("z", "eb", 7, 1), ("z", "fb", 5, 1), ("agc", 1, 1, 1), ("z", "fy", 5, 0), ("z", "eb", 6, 0),
+    ("age", 1, 1, 0), ("z", "fy", 4, 1), ("z", "upb", 7, 0), ("age", 1, 1, 1), ("z", "upb", 8, 1), ("z", "fy", 6, 0),
+    ("agb", 1, 0, 0), ("agb", 1, 0, 1), ("z", "eb", 8, 1), ("z", "eb", 7, 0), ("z", "fb", 5, 0), ("z", "upb", 8, 0),
+    ("agd", 1, 1), ("agc", 1, 0, 1), ("z", "fy", 5, 1), ("z", "fb", 6, 1), ("z", "upb", 9, 1), ("agc", 1, 0, 0),
+    ("z", "fy", 7, 0), ("yd", "upy"), ("ffup", 1), ("z", "eb", 9, 1), ("age", 1, 0, 1), ("yd", "ey"),
+    ("z", "eb", 8, 0), ("z", "fy", 6, 1), ("rsa", 1, 0), ("age", 1, 0, 0), ("z", "fb", 6, 0), ("rsa", 1, 1),
+    ("z", "fb", 7, 1), ("rsb", 1, 0), ("z", "fy", 8, 0), ("agd", 1, 0), ("rsb", 1, 1), ("z", "fy", 7, 1), ("ffup", 0),
+    ("z", "fy", 9, 0), ("z", "fb", 8, 1), ("z", "fb", 7, 0), ("rsc", 1, 1), ("rsc", 1, 0), ("z", "fy", 8, 1),
+    ("rsa", 0, 0), ("rsa", 0, 1), ("rsb", 0, 0), ("rsb", 0, 1), ("yd", "fy"), ("z", "fb", 9, 1), ("z", "fb", 8, 0),
+    ("rsa", 2, 0), ("rsd", 1), ("rsb", 2, 0), ("rsa", 3, 0), ("rsc", 0, 0), ("rsc", 0, 1), ("rsa", 2, 1),
+    ("rsb", 3, 0), ("rsb", 2, 1), ("rsc", 2, 0), ("rsa", 3, 1), ("rsc", 2, 1), ("rsb", 3, 1), ("rsd", 0),
+    ("rsc", 3, 1), ("rsc", 3, 0), ("rsd", 2), ("rsd", 3),
 )
 
 
@@ -62,8 +69,8 @@
     x_ref, g1_ref, wu_ref, wv_ref, su_ref, sv_ref, mg_ref, sw_ref, sb_ref, wo_ref, so_ref,
     g2_ref, wup_ref, sup_ref, wdn_ref, sdn_ref,
     out_ref,
-    wuv, wout, wup, wdn, xg, rg, gg, wmix, ub, vt, st_own, st_p, st_c, st_x, hid,
-    ps, pr, qs, op, fi, mask, bias,
+    wuv, wout, wup, wdn, xg, rg, gg, wmix, ub, vt, st, hid,
+    ps, pr, qs, op, fi, mask, bias, total_e,
     z_recv, z_send, y_recv, y_send, ag_recv, ag_send, agp_recv, agp_send,
     rp_recv, rp_send, rr_recv, rr_send, st_recv, st_send, a2_recv, a2_send,
 ):
@@ -151,8 +158,10 @@
         return result
 
     streams = {}
+    dn_half = k_fs // 2
     for s in (make("uv", wuv, False, 0, k_fs, SWAP["uv"]) + make("out", wout, True, 0, u_w, SWAP["out"])
-              + make("up", wup, False, 0, k_fs, SWAP["up"]) + make("dn", wdn, True, 0, h_w, SWAP["dn"])):
+              + make("up", wup, False, 0, k_fs, SWAP["up"]) + make("e", wdn, False, 0, dn_half, SWAP["e"])
+              + make("f", wdn, False, dn_half, dn_half, SWAP["f"])):
         s.index = len(streams)
         streams[s.name] = s
 
@@ -265,21 +274,28 @@
 
     PAIRS = ((2, 1), (3, 0))
 
-    def product(k, rel, c):
-        j = chip(rel) * CORES + c
-        right = jnp.concatenate([wdn[2 * j], wdn[2 * j + 1]], axis=1)
-        return jnp.dot(hid[pl.ds(k * chunk, chunk), :], right, preferred_element_type=F32)
+    def product(u, rels, c):
+        k, e = u % CHUNKS, u // CHUNKS
+        parts = []
+        for rel in rels:
+            j = chip(rel) * CORES + c
+            for shard in (2 * j, 2 * j + 1):
+                at = pl.multiple_of(shard * k_fs + e * dn_half, dn_half)
+                parts.append(wdn[pl.ds(at, dn_half), :])
+        both = lax.dot_general(hid[pl.ds(k * chunk, chunk), :], jnp.concatenate(parts, axis=0),
+                               (((1,), (1,)), ((), ())), preferred_element_type=F32)
+        return (rels[0], both[:, :k_fs]), (rels[1], both[:, k_fs:])
 
     def rs_a(k, p):
-        for rel in PAIRS[p]:
-            ps[k, rel] = product(k, rel, 1 - core).astype(BF)
+        for rel, value in product(k, PAIRS[p], 1 - core):
+            ps[k, rel] = value.astype(BF)
             rcopy(ps.at[k, rel], pr.at[k, rel], rp_send.at[k], rp_recv.at[k, rel], to_mate).start()
 
     def rs_b(k, p):
         ss = rr_send.at[k]
-        for rel in PAIRS[p]:
+        for rel, value in product(k, PAIRS[p], core):
             got(pr.at[k, rel], rp_recv.at[k, rel], rp_send.at[k], to_mate)
-            qs[k, rel] = (product(k, rel, core) + pr[k, rel].astype(F32)).astype(BF)
+            qs[k, rel] = (value + pr[k, rel].astype(F32)).astype(BF)
             low, high = qs.at[k, rel, pl.ds(0, half), :], qs.at[k, rel, pl.ds(half, half), :]
             if rel == 2:
                 rcopy(low, op.at[0, k], ss, rr_recv.at[k, 0], to_right).start()
@@ -302,9 +318,14 @@
         for n, side, lo in ((2, 0, half), (3, 1, 0), (4, 0, 0), (5, 1, half)):
             got(fi.at[side, k, pl.ds(lo, half), :], rr_recv.at[k, n], ss, to_right)
         for r in range(0, chunk, ROWS):
-            rows, at = pl.ds(r, ROWS), pl.ds(k * chunk + r, ROWS)
+            rows, at = pl.ds(r, ROWS), pl.ds((k % CHUNKS) * chunk + r, ROWS)
             total = qs[k, 0, rows, :].astype(F32) + fi[0, k, rows, :].astype(F32) + fi[1, k, rows, :].astype(F32)
-            out_ref[at, :] = (rg[t, at, :].astype(F32) + total).astype(BF)
+            if k < CHUNKS:
+                total_e[at, :] = total
+            else:
+                first, h = total_e[at, :], dn_half
+                total = jnp.concatenate([first[:, :h], total[:, :h], first[:, h:], total[:, h:]], axis=1)
+                out_ref[at, :] = (rg[t, at, :].astype(F32) + total).astype(BF)
 
     def column(row):
         return jnp.broadcast_to(row, (row.shape[1], row.shape[1])).T
@@ -328,28 +349,27 @@
             ub[pl.ds(at, ROWS), :] = act[:, :u_w]
             turned = act[:, u_w:].T
             vt[:, pl.ds(at, ROWS)] = turned
-            st_own[k, :, pl.ds(r, ROWS)] = jnp.concatenate(
-                [jnp.sum(turned, axis=0, keepdims=True), jnp.sum(turned * turned, axis=0, keepdims=True),
-                 jnp.zeros((6, ROWS), F32)], axis=0)
-        rcopy(st_own.at[k], st_p.at[k], st_send.at[k], st_recv.at[k, 3], to_mate).start()
-
-    def stats(k):
-        got(st_p.at[k], st_recv.at[k, 3], st_send.at[k], to_mate)
-        st_c[k] = st_own[k] + st_p[k]
-        for n, to in enumerate((to_right, to_left, to_opp)):
-            rcopy(st_c.at[k], st_x.at[n, k], st_send.at[k], st_recv.at[k, n], to).start()
+            for sums, first in ((jnp.sum(turned, axis=0, keepdims=True), 0),
+                                (jnp.sum(turned * turned, axis=0, keepdims=True), chunk // block)):
+                for b in range(0, ROWS, block):
+                    st[t, k, pl.ds(first + (r + b) // block, 1), :] = sums[:, b:b + block]
+        for to in others:
+            rcopy(st.at[t, k], st.at[t, k], st_send.at[k], st_recv.at[k], to).start()
 
     def mixing(k):
-        for n in range(3):
-            got(st_x.at[n, k], st_recv.at[k, n], st_send.at[k], to_mate)
-        total = st_c[k] + st_x[0, k] + st_x[1, k] + st_x[2, k]
-        mean = total[0:1] / gm_w
-        square = total[1:2] / gm_w
+        got(st.at[pl.ds(0, n_tp - 1), k], st_recv.at[k], st_send.at[k], to_mate)
+        total = st[0, k]
+        for n in range(1, n_tp):
+            total = total + st[n, k]
+        blocks = chunk // block
+        mean = total[:blocks] / gm_w
+        square = total[blocks:2 * blocks] / gm_w
         scale = lax.rsqrt(square - mean * mean + EPS)
         gain = column(mg_ref[...])[:, 0:1]
         for b in range(0, chunk, block):
             at = k * chunk + b
-            v_norm = ((vt[:, pl.ds(at, block)] - mean[:, b:b + block]) * scale[:, b:b + block] * gain).astype(BF)
+            n = b // block
+            v_norm = ((vt[:, pl.ds(at, block)] - mean[n:n + 1]) * scale[n:n + 1] * gain).astype(BF)
             mixed = lax.dot_general(mask[...], v_norm, (((1,), (1,)), ((), ())), preferred_element_type=F32)
             gg[t, pl.ds(at, block), :] = (ub[pl.ds(at, block), :] * (mixed + bias[...])).astype(BF)
 
@@ -377,7 +397,7 @@
             g2 = column(g2_ref[pl.ds(f, 1), :])[:, 0:1]
             wup[own, :] = (rounded(wup_ref[...]) * g2).astype(BF)
         else:
-            wdn[f] = (rounded(wdn_ref[...]) * sdn_ref[...]).astype(BF)
+            wdn[own, :] = (rounded(wdn_ref[...]) * sdn_ref[...]).T.astype(BF)
             xg[t] = x_ref[...]
             at = lax.broadcasted_iota(jnp.int32, (block, block), 0)
             low = at >= lax.broadcasted_iota(jnp.int32, (block, block), 1)
@@ -387,7 +407,7 @@
 
     steps = {
         "prep": prep, "z": z_hop, "fe": z_even, "fo": z_odd, "yd": y_done, "aga": ag_a, "agb": ag_b, "agc": ag_c,
-        "age": ag_e, "agd": ag_d, "gating": gating, "stats": stats, "mixing": mixing, "a2s": a2_s, "a2w": a2_w,
+        "age": ag_e, "agd": ag_d, "gating": gating, "mixing": mixing, "a2s": a2_s, "a2w": a2_w,
         "outp": out_p, "ffup": ff_up, "rsa": rs_a, "rsb": rs_b, "rsc": rs_c, "rsd": rs_d,
     }
     for name, *rest in ORDER:
@@ -402,10 +422,11 @@
             rows = pl.ds(k * chunk, chunk)
             sent(buf.at[pl.ds(0, 3), rows, :], ag_send.at[ph, k], ag_recv.at[ph, k, 0], to_right)
             sent(buf.at[pl.ds(0, n_x), rows, :], agp_send.at[ph, k], agp_recv.at[ph, k], to_mate)
+    for u in range(2 * CHUNKS):
+        sent(ps.at[u], rp_send.at[u], rp_recv.at[u, 0], to_mate)
+        sent(qs.at[u, pl.ds(0, 3)], rr_send.at[u], rr_recv.at[u, 0], to_right)
     for k in range(CHUNKS):
-        sent(ps.at[k], rp_send.at[k], rp_recv.at[k, 0], to_mate)
-        sent(qs.at[k, pl.ds(0, 3)], rr_send.at[k], rr_recv.at[k, 0], to_right)
-        sent(st_x.at[pl.ds(0, 4), k], st_send.at[k], st_recv.at[k, 0], to_mate)
+        sent(st.at[pl.ds(0, n_tp - 1), k], st_send.at[k], st_recv.at[k], to_mate)
     sent(wmix.at[pl.ds(0, n_tp - 1)], a2_send.at[0], a2_recv.at[0], to_mate)
 
 
@@ -433,29 +454,27 @@
         pltpu.VMEM((feats, 2 * u_w), BF),
         pltpu.VMEM((n_fs, u_w, o_w), BF),
         pltpu.VMEM((feats, h_w), BF),
-        pltpu.VMEM((n_fs, h_w, d_w), BF),
+        pltpu.VMEM((feats, h_w), BF),
         pltpu.VMEM((n_tp, rows, width), BF),
         pltpu.VMEM((n_tp, rows, width), BF),
         pltpu.VMEM((n_tp, rows, u_w), BF),
         pltpu.VMEM((n_tp, 2, u_w, o_w), BF),
         pltpu.VMEM((rows, u_w), F32),
         pltpu.VMEM((u_w, rows), F32),
-        pltpu.VMEM((CHUNKS, 8, chunk), F32),
-        pltpu.VMEM((CHUNKS, 8, chunk), F32),
-        pltpu.VMEM((CHUNKS, 8, chunk), F32),
-        pltpu.VMEM((4, CHUNKS, 8, chunk), F32),
+        pltpu.VMEM((n_tp, CHUNKS, 2 * chunk // block, block), F32),
         pltpu.VMEM((rows, h_w), BF),
-        pltpu.VMEM((CHUNKS, n_x, chunk, width), BF),
-        pltpu.VMEM((CHUNKS, n_x, chunk, width), BF),
-        pltpu.VMEM((CHUNKS, n_x, chunk, width), BF),
-        pltpu.VMEM((2, CHUNKS, chunk // 2, width), BF),
-        pltpu.VMEM((2, CHUNKS, chunk, width), BF),
+        pltpu.VMEM((2 * CHUNKS, n_x, chunk, d_w), BF),
+        pltpu.VMEM((2 * CHUNKS, n_x, chunk, d_w), BF),
+        pltpu.VMEM((2 * CHUNKS, n_x, chunk, d_w), BF),
+        pltpu.VMEM((2, 2 * CHUNKS, chunk // 2, d_w), BF),
+        pltpu.VMEM((2, 2 * CHUNKS, chunk, d_w), BF),
         pltpu.VMEM((block, block), BF),
         pltpu.VMEM((block, block), F32),
+        pltpu.VMEM((rows, d_w), F32),
         dma((n_streams, 2, n_fs // 2)), dma((n_streams,)), dma((n_streams,)), dma((n_streams,)),
         dma((3, CHUNKS, 6)), dma((3, CHUNKS)), dma((3, CHUNKS)), dma((3, CHUNKS)),
-        dma((CHUNKS, n_x)), dma((CHUNKS,)), dma((CHUNKS, 6)), dma((CHUNKS,)),
-        dma((CHUNKS, 4)), dma((CHUNKS,)), dma((1,)), dma((1,)),
+        dma((2 * CHUNKS, n_x)), dma((2 * CHUNKS,)), dma((2 * CHUNKS, 6)), dma((2 * CHUNKS,)),
+        dma((CHUNKS,)), dma((CHUNKS,)), dma((1,)), dma((1,)),
     ]
     vmem = pl.BlockSpec(memory_space=pltpu.VMEM)
     return pl.pallas_call(

time: 130 us -> 126 us (0.969)
  Pallas kernels: 128 us -> 124 us
    pallas_call x1, Pallas kernels: 128 us -> 124 us  [per_device(): pl.pallas_call(functools.partial(kernel, dims), out_shape=jax.ShapeDtypeS...]
where the time goes in v4:
time: 126 us
  Pallas kernels  124 us (98%)
  local copies, waits for them, and re-layouts  1.87 us (1%)
    pallas_call x1, Pallas kernels, per_device(): pl.pallas_call(functools.partial(kernel, dims), out_shape=jax.ShapeDtypeS...  124 us

profile of v4, /device:TPU:33, one launch (start us, length us, event | category | flops | bytes accessed | tf_op | source)
XLA Modules:
  0.0 126.3 jit_solution(13862828530152261589)
XLA Ops:
  0.0 124.4 %layer.1 = bf16[1024,256]{1,0:T(8,128)(2,1)} custom-call(bf16[1024,256]{1,0:T(8,128)(2,1)} %x_ref.1, f32[16,128]{1,0:T(8,128)} %bitcast.8, f32[128,128]{1,0:T(8,128)} %wu_ref.1, f32[128,128]{1,0:T(8,128)} %wv_ref.1, f32[1,128]{1,0:T(1,128)} %bitcast.11, f32[1,128]{1,0:T(1,128)} %bitcast.12, f32[1,128]{1,0:T(1,128)} %bitcast.13, f32[4,128,128]{2,1,0:T(8,128)} %sw_ref.1, ...), custom_call_target="tpu_custom_call" | custom-call | tf_op jit(solution)/shard_map/layer/pallas_call | solution.py:480
  124.4 1.9 %copy.18 = bf16[1024,256]{1,0:T(8,128)(2,1)} copy(bf16[1024,256]{1,0:T(8,128)(2,1)} %layer.1) | data formatting | bytes 1048576

commit v5 on v4

--- a/solution.py
+++ b/solution.py
@@ -14,48 +14,49 @@
 CORES = 2
 CHUNKS = 2
 ROWS = 256
+INPUTS = 16
 SWAP = {"uv": 64, "out": 64, "up": 48, "e": 16, "f": 16}
 ORDER = (
-    ("prep", 0), ("z", "outy", 1, 0), ("aga", 0, 1), ("z", "outy", 1, 1), ("fe", "uvy", 1, 0), ("prep", 1),
-    ("z", "upy", 1, 0), ("fe", "uvy", 1, 1), ("prep", 2), ("z", "outy", 2, 1), ("z", "outy", 2, 0), ("aga", 0, 0),
-    ("z", "upb", 1, 1), ("z", "ey", 1, 1), ("fo", "uvy", 2, 0), ("fe", "uvy", 2, 0), ("agb", 0, 1, 0),
-    ("z", "outy", 3, 1), ("agb", 0, 1, 1), ("fo", "uvy", 2, 1), ("fe", "uvy", 2, 1), ("z", "upy", 2, 0),
-    ("z", "upy", 1, 1), ("z", "outy", 4, 1), ("z", "outy", 3, 0), ("fe", "uvy", 3, 0), ("fe", "uvy", 3, 1),
-    ("agb", 0, 0, 1), ("fo", "uvy", 3, 1), ("fo", "uvy", 3, 0), ("z", "upb", 1, 0), ("z", "outy", 4, 0),
-    ("z", "ey", 1, 0), ("z", "outy", 5, 1), ("agc", 0, 1, 0), ("z", "eb", 1, 1), ("fo", "uvy", 4, 0),
-    ("agb", 0, 0, 0), ("fe", "uvy", 4, 0), ("z", "ey", 2, 1), ("agc", 0, 0, 1), ("fo", "uvy", 4, 1),
-    ("fe", "uvy", 4, 1), ("z", "outy", 5, 0), ("z", "outy", 6, 1), ("z", "upb", 2, 1), ("z", "upb", 2, 0),
-    ("z", "eb", 1, 0), ("z", "fb", 1, 1), ("fo", "uvy", 5, 1), ("age", 0, 1, 1), ("fe", "uvy", 5, 0),
-    ("agc", 0, 1, 1), ("fo", "uvy", 5, 0), ("age", 0, 1, 0), ("z", "outy", 7, 1), ("z", "outy", 6, 0),
-    ("age", 0, 0, 0), ("z", "upy", 3, 0), ("z", "ey", 3, 1), ("z", "upy", 2, 1), ("agc", 0, 0, 0),
-    ("z", "outy", 8, 1), ("z", "eb", 2, 1), ("agd", 0, 1), ("age", 0, 0, 1), ("z", "ey", 2, 0), ("z", "outy", 7, 0),
-    ("z", "fb", 1, 0), ("z", "upb", 3, 1), ("z", "upb", 3, 0), ("yd", "uvy"), ("gating", 1), ("agd", 0, 0),
-    ("gating", 0), ("z", "outy", 9, 1), ("z", "outy", 8, 0), ("z", "upy", 3, 1), ("z", "fb", 2, 1), ("z", "ey", 3, 0),
-    ("z", "upy", 4, 0), ("z", "eb", 2, 0), ("mixing", 1), ("aga", 2, 1), ("z", "fy", 1, 0), ("z", "ey", 4, 0),
-    ("z", "eb", 3, 1), ("mixing", 0), ("z", "upy", 4, 1), ("yd", "outy"), ("z", "ey", 4, 1), ("aga", 2, 0),
-    ("z", "upy", 5, 0), ("agb", 2, 1, 0), ("z", "fy", 1, 1), ("a2s",), ("z", "eb", 4, 1), ("agb", 2, 1, 1),
-    ("z", "upb", 4, 0), ("z", "eb", 3, 0), ("z", "ey", 5, 0), ("z", "upy", 5, 1), ("z", "upy", 6, 0),
-    ("z", "fb", 3, 1), ("z", "ey", 5, 1), ("agc", 2, 1, 1), ("z", "upb", 4, 1), ("z", "eb", 4, 0), ("z", "ey", 6, 0),
-    ("agc", 2, 1, 0), ("z", "fb", 2, 0), ("z", "upy", 6, 1), ("age", 2, 1, 0), ("agb", 2, 0, 1), ("agc", 2, 0, 1),
-    ("z", "ey", 6, 1), ("age", 2, 1, 1), ("z", "upy", 7, 0), ("agb", 2, 0, 0), ("agd", 2, 1), ("z", "ey", 7, 0),
-    ("z", "upb", 5, 1), ("age", 2, 0, 1), ("z", "fy", 2, 0), ("z", "upb", 5, 0), ("z", "upy", 7, 1),
-    ("z", "ey", 7, 1), ("a2w",), ("outp", 1), ("agc", 2, 0, 0), ("z", "eb", 5, 1), ("aga", 1, 1), ("z", "upy", 8, 0),
-    ("age", 2, 0, 0), ("z", "upb", 6, 1), ("z", "ey", 8, 0), ("fe", "uvy", 5, 1), ("z", "fy", 3, 0), ("agd", 2, 0),
-    ("outp", 0), ("z", "fb", 4, 1), ("z", "fb", 3, 0), ("z", "upy", 8, 1), ("z", "eb", 5, 0), ("agb", 1, 1, 0),
-    ("z", "upy", 9, 0), ("agb", 1, 1, 1), ("z", "ey", 8, 1), ("aga", 1, 0), ("z", "fy", 2, 1), ("z", "eb", 6, 1),
-    ("z", "ey", 9, 0), ("z", "fy", 4, 0), ("z", "upb", 6, 0), ("z", "upb", 7, 1), ("z", "fb", 4, 0), ("agc", 1, 1, 0),
-    ("z", "fy", 3, 1), ("z", "eb", 7, 1), ("z", "fb", 5, 1), ("agc", 1, 1, 1), ("z", "fy", 5, 0), ("z", "eb", 6, 0),
-    ("age", 1, 1, 0), ("z", "fy", 4, 1), ("z", "upb", 7, 0), ("age", 1, 1, 1), ("z", "upb", 8, 1), ("z", "fy", 6, 0),
-    ("agb", 1, 0, 0), ("agb", 1, 0, 1), ("z", "eb", 8, 1), ("z", "eb", 7, 0), ("z", "fb", 5, 0), ("z", "upb", 8, 0),
-    ("agd", 1, 1), ("agc", 1, 0, 1), ("z", "fy", 5, 1), ("z", "fb", 6, 1), ("z", "upb", 9, 1), ("agc", 1, 0, 0),
-    ("z", "fy", 7, 0), ("yd", "upy"), ("ffup", 1), ("z", "eb", 9, 1), ("age", 1, 0, 1), ("yd", "ey"),
-    ("z", "eb", 8, 0), ("z", "fy", 6, 1), ("rsa", 1, 0), ("age", 1, 0, 0), ("z", "fb", 6, 0), ("rsa", 1, 1),
-    ("z", "fb", 7, 1), ("rsb", 1, 0), ("z", "fy", 8, 0), ("agd", 1, 0), ("rsb", 1, 1), ("z", "fy", 7, 1), ("ffup", 0),
-    ("z", "fy", 9, 0), ("z", "fb", 8, 1), ("z", "fb", 7, 0), ("rsc", 1, 1), ("rsc", 1, 0), ("z", "fy", 8, 1),
-    ("rsa", 0, 0), ("rsa", 0, 1), ("rsb", 0, 0), ("rsb", 0, 1), ("yd", "fy"), ("z", "fb", 9, 1), ("z", "fb", 8, 0),
-    ("rsa", 2, 0), ("rsd", 1), ("rsb", 2, 0), ("rsa", 3, 0), ("rsc", 0, 0), ("rsc", 0, 1), ("rsa", 2, 1),
-    ("rsb", 3, 0), ("rsb", 2, 1), ("rsc", 2, 0), ("rsa", 3, 1), ("rsc", 2, 1), ("rsb", 3, 1), ("rsd", 0),
-    ("rsc", 3, 1), ("rsc", 3, 0), ("rsd", 2), ("rsd", 3),
+    ("prep", 0), ("z", "outy", 1, 0), ("fe", "uvy", 1, 0), ("aga", 0, 0), ("z", "outy", 1, 1), ("fe", "uvy", 1, 1),
+    ("prep", 1), ("z", "upy", 1, 0), ("z", "outy", 2, 0), ("z", "upb", 1, 1), ("prep", 2), ("z", "ey", 1, 1),
+    ("z", "outy", 2, 1), ("fo", "uvy", 2, 0), ("fe", "uvy", 2, 0), ("aga", 0, 1), ("fo", "uvy", 2, 1),
+    ("fe", "uvy", 2, 1), ("z", "upy", 2, 0), ("z", "outy", 3, 0), ("z", "eb", 1, 1), ("agb", 0, 0, 0),
+    ("z", "outy", 3, 1), ("z", "ey", 2, 1), ("fe", "uvy", 3, 0), ("fe", "uvy", 3, 1), ("agb", 0, 1, 1),
+    ("z", "ey", 1, 0), ("agb", 0, 0, 1), ("fo", "uvy", 3, 0), ("z", "outy", 4, 0), ("z", "fb", 1, 0),
+    ("fo", "uvy", 3, 1), ("z", "outy", 4, 1), ("z", "fy", 1, 1), ("agc", 0, 0, 0), ("z", "eb", 2, 1),
+    ("fo", "uvy", 4, 1), ("fe", "uvy", 4, 0), ("fe", "uvy", 4, 1), ("agb", 0, 1, 0), ("z", "outy", 5, 1),
+    ("z", "outy", 5, 0), ("z", "upy", 1, 1), ("z", "upb", 1, 0), ("fo", "uvy", 4, 0), ("z", "fb", 1, 1),
+    ("z", "eb", 1, 0), ("age", 0, 1, 1), ("fo", "uvy", 5, 1), ("fo", "uvy", 5, 0), ("age", 0, 0, 0),
+    ("fe", "uvy", 5, 0), ("z", "outy", 6, 1), ("agc", 0, 1, 1), ("agc", 0, 1, 0), ("z", "ey", 3, 1),
+    ("z", "outy", 6, 0), ("z", "ey", 2, 0), ("z", "upy", 3, 0), ("age", 0, 0, 1), ("z", "upy", 2, 1),
+    ("agc", 0, 0, 1), ("z", "outy", 7, 1), ("z", "upb", 2, 1), ("z", "outy", 7, 0), ("z", "eb", 2, 0),
+    ("age", 0, 1, 0), ("yd", "uvy"), ("agd", 0, 0), ("gating", 0), ("agd", 0, 1), ("z", "ey", 3, 0),
+    ("z", "eb", 3, 1), ("gating", 1), ("z", "outy", 8, 1), ("z", "upy", 3, 1), ("z", "upy", 4, 0), ("z", "upb", 2, 0),
+    ("z", "outy", 8, 0), ("z", "upb", 3, 1), ("mixing", 0), ("z", "outy", 9, 1), ("z", "fb", 2, 1),
+    ("fe", "uvy", 5, 1), ("aga", 2, 0), ("z", "eb", 3, 0), ("mixing", 1), ("z", "upy", 5, 0), ("z", "ey", 4, 0),
+    ("z", "upy", 4, 1), ("aga", 2, 1), ("agb", 2, 0, 1), ("agb", 2, 0, 0), ("z", "eb", 4, 0), ("z", "upb", 3, 0),
+    ("z", "fy", 2, 1), ("z", "eb", 4, 1), ("z", "ey", 4, 1), ("z", "upy", 6, 0), ("z", "upy", 5, 1),
+    ("z", "upb", 4, 1), ("agb", 2, 1, 1), ("yd", "outy"), ("a2s",), ("agb", 2, 1, 0), ("z", "eb", 5, 1),
+    ("agc", 2, 0, 0), ("z", "ey", 5, 0), ("age", 2, 0, 1), ("z", "fy", 1, 0), ("z", "fb", 2, 0), ("z", "upy", 7, 0),
+    ("z", "ey", 5, 1), ("agc", 2, 0, 1), ("z", "upy", 6, 1), ("z", "ey", 6, 0), ("age", 2, 0, 0), ("z", "upb", 4, 0),
+    ("z", "upb", 5, 1), ("age", 2, 1, 1), ("z", "fy", 2, 0), ("z", "fb", 3, 1), ("z", "upy", 8, 0), ("z", "ey", 7, 0),
+    ("z", "upy", 7, 1), ("z", "ey", 6, 1), ("a2w",), ("agd", 2, 0), ("outp", 0), ("aga", 1, 0), ("z", "upb", 6, 1),
+    ("z", "upb", 5, 0), ("agc", 2, 1, 0), ("agc", 2, 1, 1), ("age", 2, 1, 0), ("z", "eb", 6, 1), ("z", "eb", 5, 0),
+    ("agd", 2, 1), ("outp", 1), ("z", "upy", 9, 0), ("z", "upy", 8, 1), ("z", "ey", 8, 0), ("z", "ey", 7, 1),
+    ("z", "fy", 3, 0), ("z", "fb", 3, 0), ("z", "fb", 4, 1), ("agb", 1, 0, 0), ("z", "upb", 7, 1), ("z", "upb", 6, 0),
+    ("agb", 1, 0, 1), ("z", "ey", 9, 0), ("z", "ey", 8, 1), ("z", "fy", 4, 0), ("z", "fy", 3, 1), ("z", "eb", 6, 0),
+    ("z", "eb", 7, 1), ("aga", 1, 1), ("agc", 1, 0, 1), ("z", "fb", 4, 0), ("z", "fb", 5, 1), ("agc", 1, 0, 0),
+    ("z", "fy", 5, 0), ("z", "fy", 4, 1), ("age", 1, 0, 1), ("z", "upb", 8, 1), ("age", 1, 0, 0), ("z", "upb", 7, 0),
+    ("z", "eb", 8, 1), ("agb", 1, 1, 1), ("agb", 1, 1, 0), ("z", "eb", 7, 0), ("z", "fy", 6, 0), ("agd", 1, 0),
+    ("z", "fy", 5, 1), ("z", "fb", 6, 1), ("yd", "upy"), ("z", "upb", 9, 1), ("z", "fb", 5, 0), ("z", "upb", 8, 0),
+    ("ffup", 0), ("z", "fy", 6, 1), ("z", "fy", 7, 0), ("agc", 1, 1, 0), ("z", "eb", 9, 1), ("z", "eb", 8, 0),
+    ("yd", "ey"), ("agc", 1, 1, 1), ("age", 1, 1, 1), ("rsa", 0, 0), ("z", "fb", 6, 0), ("age", 1, 1, 0),
+    ("z", "fb", 7, 1), ("rsa", 0, 1), ("rsb", 0, 0), ("agd", 1, 1), ("z", "fy", 7, 1), ("z", "fy", 8, 0),
+    ("rsb", 0, 1), ("ffup", 1), ("z", "fb", 8, 1), ("z", "fb", 7, 0), ("z", "fy", 9, 0), ("z", "fy", 8, 1),
+    ("rsc", 0, 1), ("rsc", 0, 0), ("rsa", 1, 0), ("rsa", 1, 1), ("rsb", 1, 0), ("rsb", 1, 1), ("z", "fb", 9, 1),
+    ("z", "fb", 8, 0), ("yd", "fy"), ("rsa", 2, 0), ("rsd", 0), ("rsb", 2, 0), ("rsa", 3, 1), ("rsc", 1, 1),
+    ("rsa", 3, 0), ("rsb", 3, 1), ("rsc", 1, 0), ("rsb", 3, 0), ("rsa", 2, 1), ("rsb", 2, 1), ("rsc", 2, 0),
+    ("rsc", 2, 1), ("rsd", 1), ("rsc", 3, 0), ("rsc", 3, 1), ("rsd", 2), ("rsd", 3),
 )
 
 
@@ -66,14 +67,18 @@
 
 def kernel(
     dims,
-    x_ref, g1_ref, wu_ref, wv_ref, su_ref, sv_ref, mg_ref, sw_ref, sb_ref, wo_ref, so_ref,
-    g2_ref, wup_ref, sup_ref, wdn_ref, sdn_ref,
-    out_ref,
-    wuv, wout, wup, wdn, xg, rg, gg, wmix, ub, vt, st, hid,
-    ps, pr, qs, op, fi, mask, bias, total_e,
-    z_recv, z_send, y_recv, y_send, ag_recv, ag_send, agp_recv, agp_send,
-    rp_recv, rp_send, rr_recv, rr_send, st_recv, st_send, a2_recv, a2_send,
+    *refs,
 ):
+    given, out_ref, held, (
+        wuv, wout, wup, wdn, xg, rg, gg, wmix, ub, vt, st, hid,
+        ps, pr, qs, op, fi, mask, bias, total_e,
+        z_recv, z_send, y_recv, y_send, ag_recv, ag_send, agp_recv, agp_send,
+        rp_recv, rp_send, rr_recv, rr_send, st_recv, st_send, a2_recv, a2_send, in_sem,
+    ) = refs[:INPUTS], refs[INPUTS], refs[INPUTS + 1:2 * INPUTS + 1], refs[2 * INPUTS + 1:]
+    (
+        x_ref, g1_ref, wu_ref, wv_ref, su_ref, sv_ref, mg_ref, sw_ref, sb_ref, wo_ref, so_ref,
+        g2_ref, wup_ref, sup_ref, wdn_ref, sdn_ref,
+    ) = held
     n_fs, n_tp = dims["fs"], dims["tp"]
     n_x = n_tp // CORES
     half_ring = n_fs // 2
@@ -114,7 +119,17 @@
     barrier = pltpu.get_barrier_semaphore()
     for n in neighbours:
         pl.semaphore_signal(barrier, inc=1, device_id=n, device_id_type=MESH)
+    loads = [pltpu.make_async_copy(a, b, in_sem.at[n]) for n, (a, b) in enumerate(zip(given, held))]
+    for load in loads:
+        load.start()
     pl.semaphore_wait(barrier, len(neighbours))
+    waiting = set(range(INPUTS))
+
+    def need(*numbers):
+        for n in numbers:
+            if n in waiting:
+                waiting.discard(n)
+                loads[n].wait()
 
     def rcopy(src, dst, ss, rs, dev):
         return pltpu.make_async_remote_copy(
@@ -223,6 +238,7 @@
         rcopy(piece, piece, agp_send.at[ph, k], agp_recv.at[ph, k], to_mate).start()
 
     def ag_a(ph, k):
+        need(0)
         buf = gathered[ph]
 
         def src(at, n):
@@ -390,13 +406,16 @@
 
     def prep(n):
         if n == 0:
+            need(1, 2, 3, 9, 10)
             g1 = column(g1_ref[pl.ds(f, 1), :])
             wuv[own, :] = (jnp.concatenate([rounded(wu_ref[...]) * g1, rounded(wv_ref[...]) * g1], axis=1)).astype(BF)
             wout[f] = (rounded(wo_ref[...]) * so_ref[...]).astype(BF)
         elif n == 1:
+            need(11, 12)
             g2 = column(g2_ref[pl.ds(f, 1), :])[:, 0:1]
             wup[own, :] = (rounded(wup_ref[...]) * g2).astype(BF)
         else:
+            need(*range(INPUTS))
             wdn[own, :] = (rounded(wdn_ref[...]) * sdn_ref[...]).T.astype(BF)
             xg[t] = x_ref[...]
             at = lax.broadcasted_iota(jnp.int32, (block, block), 0)
@@ -451,6 +470,7 @@
     dma = pltpu.SemaphoreType.DMA
     n_streams = 8
     scratch = [
+        *[pltpu.VMEM(a.shape, a.dtype) for a in args],
         pltpu.VMEM((feats, 2 * u_w), BF),
         pltpu.VMEM((n_fs, u_w, o_w), BF),
         pltpu.VMEM((feats, h_w), BF),
@@ -474,13 +494,13 @@
         dma((n_streams, 2, n_fs // 2)), dma((n_streams,)), dma((n_streams,)), dma((n_streams,)),
         dma((3, CHUNKS, 6)), dma((3, CHUNKS)), dma((3, CHUNKS)), dma((3, CHUNKS)),
         dma((2 * CHUNKS, n_x)), dma((2 * CHUNKS,)), dma((2 * CHUNKS, 6)), dma((2 * CHUNKS,)),
-        dma((CHUNKS,)), dma((CHUNKS,)), dma((1,)), dma((1,)),
+        dma((CHUNKS,)), dma((CHUNKS,)), dma((1,)), dma((1,)), dma((INPUTS,)),
     ]
     vmem = pl.BlockSpec(memory_space=pltpu.VMEM)
     return pl.pallas_call(
         functools.partial(kernel, dims),
         out_shape=jax.ShapeDtypeStruct(tokens.shape, tokens.dtype),
-        in_specs=[vmem] * len(args),
+        in_specs=[pl.BlockSpec(memory_space=pltpu.HBM)] * len(args),
         out_specs=vmem,
         scratch_shapes=scratch,
         name="layer",

time: 126 us -> 124 us (0.984)
  Pallas kernels: 124 us -> 122 us
    pallas_call x1, Pallas kernels: 124 us -> 122 us  [per_device(): pl.pallas_call(functools.partial(kernel, dims), out_shape=jax.ShapeDtypeS...]
where the time goes in v5:
time: 124 us
  Pallas kernels  122 us (98%)
  local copies, waits for them, and re-layouts  1.87 us (2%)
    pallas_call x1, Pallas kernels, per_device(): pl.pallas_call(functools.partial(kernel, dims), out_shape=jax.ShapeDtypeS...  122 us

profile of v5, /device:TPU:33, one launch (start us, length us, event | category | flops | bytes accessed | tf_op | source)
XLA Modules:
  0.0 124.0 jit_solution(1528599654509881129)
XLA Ops:
  0.0 122.1 %layer.1 = bf16[1024,256]{1,0:T(8,128)(2,1)} custom-call(bf16[1024,256]{1,0:T(8,128)(2,1)} %refs_0_.1, f32[16,128]{1,0:T(8,128)} %bitcast.8, f32[128,128]{1,0:T(8,128)} %refs_2_.1, f32[128,128]{1,0:T(8,128)} %refs_3_.1, f32[1,128]{1,0:T(1,128)} %bitcast.11, f32[1,128]{1,0:T(1,128)} %bitcast.12, f32[1,128]{1,0:T(1,128)} %bitcast.13, f32[4,128,128]{2,1,0:T(8,128)} %refs_7_.1, ...), custom_call_target="tpu_custom_call" | custom-call | tf_op jit(solution)/shard_map/layer/pallas_call | solution.py:500
  122.1 1.9 %copy.18 = bf16[1024,256]{1,0:T(8,128)(2,1)} copy(bf16[1024,256]{1,0:T(8,128)(2,1)} %layer.1) | data formatting | bytes 1048576

commit v6 on v5

--- a/solution.py
+++ b/solution.py
@@ -17,46 +17,45 @@
 INPUTS = 16
 SWAP = {"uv": 64, "out": 64, "up": 48, "e": 16, "f": 16}
 ORDER = (
-    ("prep", 0), ("z", "outy", 1, 0), ("fe", "uvy", 1, 0), ("aga", 0, 0), ("z", "outy", 1, 1), ("fe", "uvy", 1, 1),
-    ("prep", 1), ("z", "upy", 1, 0), ("z", "outy", 2, 0), ("z", "upb", 1, 1), ("prep", 2), ("z", "ey", 1, 1),
-    ("z", "outy", 2, 1), ("fo", "uvy", 2, 0), ("fe", "uvy", 2, 0), ("aga", 0, 1), ("fo", "uvy", 2, 1),
-    ("fe", "uvy", 2, 1), ("z", "upy", 2, 0), ("z", "outy", 3, 0), ("z", "eb", 1, 1), ("agb", 0, 0, 0),
-    ("z", "outy", 3, 1), ("z", "ey", 2, 1), ("fe", "uvy", 3, 0), ("fe", "uvy", 3, 1), ("agb", 0, 1, 1),
-    ("z", "ey", 1, 0), ("agb", 0, 0, 1), ("fo", "uvy", 3, 0), ("z", "outy", 4, 0), ("z", "fb", 1, 0),
-    ("fo", "uvy", 3, 1), ("z", "outy", 4, 1), ("z", "fy", 1, 1), ("agc", 0, 0, 0), ("z", "eb", 2, 1),
-    ("fo", "uvy", 4, 1), ("fe", "uvy", 4, 0), ("fe", "uvy", 4, 1), ("agb", 0, 1, 0), ("z", "outy", 5, 1),
-    ("z", "outy", 5, 0), ("z", "upy", 1, 1), ("z", "upb", 1, 0), ("fo", "uvy", 4, 0), ("z", "fb", 1, 1),
-    ("z", "eb", 1, 0), ("age", 0, 1, 1), ("fo", "uvy", 5, 1), ("fo", "uvy", 5, 0), ("age", 0, 0, 0),
-    ("fe", "uvy", 5, 0), ("z", "outy", 6, 1), ("agc", 0, 1, 1), ("agc", 0, 1, 0), ("z", "ey", 3, 1),
-    ("z", "outy", 6, 0), ("z", "ey", 2, 0), ("z", "upy", 3, 0), ("age", 0, 0, 1), ("z", "upy", 2, 1),
-    ("agc", 0, 0, 1), ("z", "outy", 7, 1), ("z", "upb", 2, 1), ("z", "outy", 7, 0), ("z", "eb", 2, 0),
-    ("age", 0, 1, 0), ("yd", "uvy"), ("agd", 0, 0), ("gating", 0), ("agd", 0, 1), ("z", "ey", 3, 0),
-    ("z", "eb", 3, 1), ("gating", 1), ("z", "outy", 8, 1), ("z", "upy", 3, 1), ("z", "upy", 4, 0), ("z", "upb", 2, 0),
-    ("z", "outy", 8, 0), ("z", "upb", 3, 1), ("mixing", 0), ("z", "outy", 9, 1), ("z", "fb", 2, 1),
-    ("fe", "uvy", 5, 1), ("aga", 2, 0), ("z", "eb", 3, 0), ("mixing", 1), ("z", "upy", 5, 0), ("z", "ey", 4, 0),
-    ("z", "upy", 4, 1), ("aga", 2, 1), ("agb", 2, 0, 1), ("agb", 2, 0, 0), ("z", "eb", 4, 0), ("z", "upb", 3, 0),
-    ("z", "fy", 2, 1), ("z", "eb", 4, 1), ("z", "ey", 4, 1), ("z", "upy", 6, 0), ("z", "upy", 5, 1),
-    ("z", "upb", 4, 1), ("agb", 2, 1, 1), ("yd", "outy"), ("a2s",), ("agb", 2, 1, 0), ("z", "eb", 5, 1),
-    ("agc", 2, 0, 0), ("z", "ey", 5, 0), ("age", 2, 0, 1), ("z", "fy", 1, 0), ("z", "fb", 2, 0), ("z", "upy", 7, 0),
-    ("z", "ey", 5, 1), ("agc", 2, 0, 1), ("z", "upy", 6, 1), ("z", "ey", 6, 0), ("age", 2, 0, 0), ("z", "upb", 4, 0),
-    ("z", "upb", 5, 1), ("age", 2, 1, 1), ("z", "fy", 2, 0), ("z", "fb", 3, 1), ("z", "upy", 8, 0), ("z", "ey", 7, 0),
-    ("z", "upy", 7, 1), ("z", "ey", 6, 1), ("a2w",), ("agd", 2, 0), ("outp", 0), ("aga", 1, 0), ("z", "upb", 6, 1),
-    ("z", "upb", 5, 0), ("agc", 2, 1, 0), ("agc", 2, 1, 1), ("age", 2, 1, 0), ("z", "eb", 6, 1), ("z", "eb", 5, 0),
-    ("agd", 2, 1), ("outp", 1), ("z", "upy", 9, 0), ("z", "upy", 8, 1), ("z", "ey", 8, 0), ("z", "ey", 7, 1),
-    ("z", "fy", 3, 0), ("z", "fb", 3, 0), ("z", "fb", 4, 1), ("agb", 1, 0, 0), ("z", "upb", 7, 1), ("z", "upb", 6, 0),
-    ("agb", 1, 0, 1), ("z", "ey", 9, 0), ("z", "ey", 8, 1), ("z", "fy", 4, 0), ("z", "fy", 3, 1), ("z", "eb", 6, 0),
-    ("z", "eb", 7, 1), ("aga", 1, 1), ("agc", 1, 0, 1), ("z", "fb", 4, 0), ("z", "fb", 5, 1), ("agc", 1, 0, 0),
-    ("z", "fy", 5, 0), ("z", "fy", 4, 1), ("age", 1, 0, 1), ("z", "upb", 8, 1), ("age", 1, 0, 0), ("z", "upb", 7, 0),
-    ("z", "eb", 8, 1), ("agb", 1, 1, 1), ("agb", 1, 1, 0), ("z", "eb", 7, 0), ("z", "fy", 6, 0), ("agd", 1, 0),
-    ("z", "fy", 5, 1), ("z", "fb", 6, 1), ("yd", "upy"), ("z", "upb", 9, 1), ("z", "fb", 5, 0), ("z", "upb", 8, 0),
-    ("ffup", 0), ("z", "fy", 6, 1), ("z", "fy", 7, 0), ("agc", 1, 1, 0), ("z", "eb", 9, 1), ("z", "eb", 8, 0),
-    ("yd", "ey"), ("agc", 1, 1, 1), ("age", 1, 1, 1), ("rsa", 0, 0), ("z", "fb", 6, 0), ("age", 1, 1, 0),
-    ("z", "fb", 7, 1), ("rsa", 0, 1), ("rsb", 0, 0), ("agd", 1, 1), ("z", "fy", 7, 1), ("z", "fy", 8, 0),
-    ("rsb", 0, 1), ("ffup", 1), ("z", "fb", 8, 1), ("z", "fb", 7, 0), ("z", "fy", 9, 0), ("z", "fy", 8, 1),
-    ("rsc", 0, 1), ("rsc", 0, 0), ("rsa", 1, 0), ("rsa", 1, 1), ("rsb", 1, 0), ("rsb", 1, 1), ("z", "fb", 9, 1),
-    ("z", "fb", 8, 0), ("yd", "fy"), ("rsa", 2, 0), ("rsd", 0), ("rsb", 2, 0), ("rsa", 3, 1), ("rsc", 1, 1),
-    ("rsa", 3, 0), ("rsb", 3, 1), ("rsc", 1, 0), ("rsb", 3, 0), ("rsa", 2, 1), ("rsb", 2, 1), ("rsc", 2, 0),
-    ("rsc", 2, 1), ("rsd", 1), ("rsc", 3, 0), ("rsc", 3, 1), ("rsd", 2), ("rsd", 3),
+    ("prep", 0), ("fe", "outy", 1, 1), ("fe", "uvy", 1, 0), ("aga", 0, 1), ("fe", "uvy", 1, 1), ("prep", 1),
+    ("aga", 0, 0), ("z", "upy", 1, 1), ("z", "upy", 1, 0), ("fe", "outy", 1, 0), ("fo", "outy", 2, 1),
+    ("fe", "outy", 2, 1), ("fo", "uvy", 2, 0), ("fe", "uvy", 2, 0), ("prep", 2), ("fe", "uvy", 2, 1),
+    ("z", "upy", 2, 0), ("z", "ey", 1, 0), ("z", "upy", 2, 1), ("fo", "uvy", 2, 1), ("z", "ey", 1, 1),
+    ("fe", "uvy", 3, 0), ("agb", 0, 0, 1), ("fe", "uvy", 3, 1), ("fe", "outy", 2, 0), ("fo", "uvy", 3, 1),
+    ("z", "upb", 1, 1), ("fo", "uvy", 3, 0), ("agb", 0, 1, 0), ("fo", "outy", 2, 0), ("z", "upb", 1, 0),
+    ("z", "fb", 1, 1), ("z", "ey", 2, 0), ("agc", 0, 0, 1), ("fe", "uvy", 4, 0), ("agb", 0, 0, 0),
+    ("fo", "uvy", 4, 0), ("agb", 0, 1, 1), ("fe", "uvy", 4, 1), ("z", "eb", 1, 0), ("fe", "outy", 3, 1),
+    ("fo", "uvy", 4, 1), ("z", "eb", 1, 1), ("agc", 0, 1, 1), ("fe", "outy", 3, 0), ("fo", "uvy", 5, 1),
+    ("agc", 0, 1, 0), ("z", "fy", 1, 0), ("z", "upb", 2, 1), ("fo", "uvy", 5, 0), ("age", 0, 0, 1), ("z", "fy", 1, 1),
+    ("agc", 0, 0, 0), ("fe", "uvy", 5, 0), ("age", 0, 1, 1), ("age", 0, 0, 0), ("z", "upy", 3, 0),
+    ("fe", "outy", 4, 1), ("z", "upy", 3, 1), ("z", "ey", 3, 0), ("age", 0, 1, 0), ("fo", "outy", 3, 1),
+    ("fe", "outy", 4, 0), ("agd", 0, 0), ("agd", 0, 1), ("z", "eb", 2, 0), ("fo", "outy", 3, 0), ("z", "upb", 3, 1),
+    ("z", "upb", 2, 0), ("yd", "uvy"), ("gating", 0), ("z", "eb", 2, 1), ("fo", "outy", 4, 1), ("gating", 1),
+    ("fe", "outy", 5, 1), ("fo", "outy", 4, 0), ("fo", "outy", 5, 0), ("fo", "outy", 5, 1), ("z", "upy", 4, 0),
+    ("z", "ey", 2, 1), ("z", "upy", 4, 1), ("z", "eb", 3, 0), ("z", "upb", 4, 1), ("mixing", 0), ("aga", 2, 0),
+    ("z", "upb", 3, 0), ("mixing", 1), ("z", "ey", 4, 0), ("z", "upy", 5, 0), ("z", "ey", 3, 1), ("aga", 2, 1),
+    ("z", "eb", 3, 1), ("z", "fb", 1, 0), ("yd", "outy"), ("z", "upy", 5, 1), ("agb", 2, 0, 0), ("z", "fy", 2, 0),
+    ("agc", 2, 0, 0), ("z", "ey", 4, 1), ("z", "ey", 5, 0), ("z", "eb", 4, 1), ("agb", 2, 0, 1), ("a2s",),
+    ("z", "upb", 5, 1), ("agb", 2, 1, 0), ("z", "upy", 6, 0), ("z", "upb", 4, 0), ("agc", 2, 0, 1), ("agb", 2, 1, 1),
+    ("z", "upy", 6, 1), ("z", "ey", 6, 0), ("z", "ey", 5, 1), ("z", "fy", 3, 0), ("z", "upy", 7, 0), ("age", 2, 0, 0),
+    ("z", "fb", 2, 1), ("age", 2, 0, 1), ("z", "upb", 5, 0), ("z", "eb", 5, 1), ("agc", 2, 1, 1), ("z", "ey", 6, 1),
+    ("z", "upy", 7, 1), ("agd", 2, 0), ("z", "ey", 7, 0), ("z", "eb", 4, 0), ("agc", 2, 1, 0), ("age", 2, 1, 1),
+    ("z", "upy", 8, 0), ("a2w",), ("outp", 0), ("aga", 1, 0), ("z", "fb", 3, 1), ("age", 2, 1, 0), ("z", "ey", 8, 0),
+    ("z", "ey", 7, 1), ("z", "upb", 6, 1), ("z", "eb", 6, 1), ("agd", 2, 1), ("outp", 1), ("z", "fb", 2, 0),
+    ("z", "upy", 8, 1), ("z", "eb", 5, 0), ("z", "upy", 9, 0), ("fe", "uvy", 5, 1), ("z", "fy", 2, 1),
+    ("z", "ey", 8, 1), ("agb", 1, 0, 1), ("z", "upb", 6, 0), ("agb", 1, 0, 0), ("z", "ey", 9, 0), ("aga", 1, 1),
+    ("z", "fy", 4, 0), ("z", "fb", 4, 1), ("z", "upb", 7, 1), ("z", "fb", 3, 0), ("z", "eb", 6, 0), ("z", "fy", 3, 1),
+    ("z", "eb", 7, 1), ("z", "fb", 5, 1), ("z", "fy", 5, 0), ("age", 1, 0, 0), ("age", 1, 0, 1), ("z", "upb", 7, 0),
+    ("z", "fy", 4, 1), ("z", "fb", 4, 0), ("z", "upb", 8, 1), ("z", "fy", 6, 0), ("agc", 1, 0, 0), ("z", "eb", 8, 1),
+    ("agb", 1, 1, 1), ("agc", 1, 0, 1), ("z", "fy", 5, 1), ("z", "fb", 6, 1), ("agb", 1, 1, 0), ("z", "eb", 7, 0),
+    ("z", "upb", 8, 0), ("agc", 1, 1, 1), ("agc", 1, 1, 0), ("agd", 1, 0), ("yd", "upy"), ("z", "upb", 9, 1),
+    ("z", "fb", 5, 0), ("ffup", 0), ("yd", "ey"), ("z", "eb", 8, 0), ("z", "fy", 6, 1), ("z", "eb", 9, 1),
+    ("z", "fy", 7, 0), ("rsa", 0), ("age", 1, 1, 0), ("z", "fb", 6, 0), ("age", 1, 1, 1), ("z", "fb", 7, 1),
+    ("rsb", 0, 0), ("rsb", 0, 1), ("z", "fy", 8, 0), ("agd", 1, 1), ("z", "fy", 7, 1), ("ffup", 1), ("z", "fb", 8, 1),
+    ("z", "fb", 7, 0), ("rsc", 0, 0), ("z", "fy", 9, 0), ("rsc", 0, 1), ("z", "fy", 8, 1), ("fe", "outy", 5, 0),
+    ("rsa", 1), ("rsb", 1, 0), ("rsb", 1, 1), ("z", "fb", 8, 0), ("z", "fb", 9, 1), ("yd", "fy"), ("rsa", 3),
+    ("rsd", 0), ("rsb", 3, 0), ("rsc", 1, 0), ("rsc", 1, 1), ("rsa", 2), ("rsb", 3, 1), ("rsb", 2, 0), ("rsc", 3, 0),
+    ("rsb", 2, 1), ("rsd", 1), ("rsc", 3, 1), ("rsc", 2, 0), ("rsc", 2, 1), ("rsd", 3), ("rsd", 2),
 )
 
 
@@ -71,7 +70,7 @@
 ):
     given, out_ref, held, (
         wuv, wout, wup, wdn, xg, rg, gg, wmix, ub, vt, st, hid,
-        ps, pr, qs, op, fi, mask, bias, total_e,
+        ps, pr, qs, op, fi, mine, mask, bias, total_e,
         z_recv, z_send, y_recv, y_send, ag_recv, ag_send, agp_recv, agp_send,
         rp_recv, rp_send, rr_recv, rr_send, st_recv, st_send, a2_recv, a2_send, in_sem,
     ) = refs[:INPUTS], refs[INPUTS], refs[INPUTS + 1:2 * INPUTS + 1], refs[2 * INPUTS + 1:]
@@ -298,20 +297,23 @@
             for shard in (2 * j, 2 * j + 1):
                 at = pl.multiple_of(shard * k_fs + e * dn_half, dn_half)
                 parts.append(wdn[pl.ds(at, dn_half), :])
-        both = lax.dot_general(hid[pl.ds(k * chunk, chunk), :], jnp.concatenate(parts, axis=0),
+        return lax.dot_general(hid[pl.ds(k * chunk, chunk), :], jnp.concatenate(parts, axis=0),
                                (((1,), (1,)), ((), ())), preferred_element_type=F32)
-        return (rels[0], both[:, :k_fs]), (rels[1], both[:, k_fs:])
-
-    def rs_a(k, p):
-        for rel, value in product(k, PAIRS[p], 1 - core):
-            ps[k, rel] = value.astype(BF)
-            rcopy(ps.at[k, rel], pr.at[k, rel], rp_send.at[k], rp_recv.at[k, rel], to_mate).start()
+
+    def rs_a(k):
+        for rels in PAIRS:
+            both = product(k, rels, 1 - core)
+            for n, rel in enumerate(rels):
+                ps[k, rel] = both[:, n * k_fs:(n + 1) * k_fs].astype(BF)
+                rcopy(ps.at[k, rel], pr.at[k, rel], rp_send.at[k], rp_recv.at[k, rel], to_mate).start()
+        for p, rels in enumerate(PAIRS):
+            mine[k, p] = product(k, rels, core)
 
     def rs_b(k, p):
         ss = rr_send.at[k]
-        for rel, value in product(k, PAIRS[p], core):
+        for n, rel in enumerate(PAIRS[p]):
             got(pr.at[k, rel], rp_recv.at[k, rel], rp_send.at[k], to_mate)
-            qs[k, rel] = (value + pr[k, rel].astype(F32)).astype(BF)
+            qs[k, rel] = (mine[k, p, :, n * k_fs:(n + 1) * k_fs] + pr[k, rel].astype(F32)).astype(BF)
             low, high = qs.at[k, rel, pl.ds(0, half), :], qs.at[k, rel, pl.ds(half, half), :]
             if rel == 2:
                 rcopy(low, op.at[0, k], ss, rr_recv.at[k, 0], to_right).start()
@@ -488,6 +490,7 @@
         pltpu.VMEM((2 * CHUNKS, n_x, chunk, d_w), BF),
         pltpu.VMEM((2, 2 * CHUNKS, chunk // 2, d_w), BF),
         pltpu.VMEM((2, 2 * CHUNKS, chunk, d_w), BF),
+        pltpu.VMEM((2 * CHUNKS, 2, chunk, 2 * d_w), F32),
         pltpu.VMEM((block, block), BF),
         pltpu.VMEM((block, block), F32),
         pltpu.VMEM((rows, d_w), F32),

time: 124 us -> 124 us (level)
  no operation moved by 1% of the time
where the time goes in v6:
time: 124 us; the launch traced here: 123 us
  Pallas kernels  122 us (98%)
  local copies, waits for them, and re-layouts  1.87 us (2%)
    pallas_call x1, Pallas kernels, per_device(): pl.pallas_call(functools.partial(kernel, dims), out_shape=jax.ShapeDtypeS...  122 us

profile of v6, /device:TPU:33, one launch (start us, length us, event | category | flops | bytes accessed | tf_op | source)
XLA Modules:
  0.0 123.4 jit_solution(11821802928446811608)
XLA Ops:
  0.0 121.5 %layer.1 = bf16[1024,256]{1,0:T(8,128)(2,1)} custom-call(bf16[1024,256]{1,0:T(8,128)(2,1)} %refs_0_.1, f32[16,128]{1,0:T(8,128)} %bitcast.8, f32[128,128]{1,0:T(8,128)} %refs_2_.1, f32[128,128]{1,0:T(8,128)} %refs_3_.1, f32[1,128]{1,0:T(1,128)} %bitcast.11, f32[1,128]{1,0:T(1,128)} %bitcast.12, f32[1,128]{1,0:T(1,128)} %bitcast.13, f32[4,128,128]{2,1,0:T(8,128)} %refs_7_.1, ...), custom_call_target="tpu_custom_call" | custom-call | tf_op jit(solution)/shard_map/layer/pallas_call | solution.py:503
  121.5 1.9 %copy.18 = bf16[1024,256]{1,0:T(8,128)(2,1)} copy(bf16[1024,256]{1,0:T(8,128)(2,1)} %layer.1) | data formatting | bytes 1048576
